TPU v7x, 128 devices: a whole 4x4x4 slice. The times are simulated.
128 devices in a mesh: sp: 16 (over z, x), tp: 4 (over y), dp: 2 (over core).
Axes of the slice: x: 4, y: 4, z: 4, core: 2. Of those that a mesh axis runs over, the one named last changes fastest.
Arguments:
- latent: bfloat16 [8192, 4, 2048], P(('sp', 'tp'), 'dp'), may hold values from -6 to 6
- context: bfloat16 [1024, 4, 2048], P('sp', 'dp'), may hold values from -6 to 6
- condition: bfloat16 [4, 2048], P('dp', 'sp'), may hold values from -6 to 6
- ctx_condition: bfloat16 [2048], P('sp'), may hold values from -6 to 6
- norm_gain: float32 [2048], replicated, may hold values from 0.1 to 1.9
- w_shift: bfloat16 [2048, 2048], P('sp', 'tp'), may hold values from -0.1875 to 0.1875
- w_scale: bfloat16 [2048, 2048], P('sp', 'tp'), may hold values from -0.1875 to 0.1875
- w_gate: bfloat16 [2048, 2048], P('sp', 'tp'), may hold values from -0.1875 to 0.1875
- w_query: bfloat16 [2048, 2048], P(None, 'tp'), may hold values from -0.125 to 0.125
- w_key: bfloat16 [2048, 512], P(None, 'tp'), may hold values from -6 to 6
- w_value: bfloat16 [2048, 512], P(None, 'tp'), may hold values from -0.125 to 0.125
- w_out: bfloat16 [2048, 2048], P('tp'), may hold values from -1 to 1
- sink: float32 [16], P('tp'), may hold values from 5 to 9
Outputs:
- mixed: bfloat16 [8192, 4, 2048], P(('sp', 'tp'), 'dp')
All inputs are finite; a program needn't handle non-finite values.
Results may differ from a plain program's by a relative error of at most 0.015.
The roundings to bfloat16 on the way count: a program that leaves them out, or rounds other values in their place, can miss the bound.
Values may be sent and summed in bfloat16 or wider, within the bound.
No kernel may reach another device: no remote copies, remote signals or barrier semaphores. Data moves between devices by JAX's collectives and lax.ppermute only.
A program may use at most 128 MiB of HBM per device.

v0:
```python
import functools

import jax
import jax.numpy as jnp
import numpy as np
from jax import lax
from jax.experimental import pallas as pl
from jax.experimental.pallas import tpu as pltpu
from jax.sharding import PartitionSpec as P


HEAD_DIM = 128
GRID_W = 64
SEQ = 8192
EPSILON = 1e-06
NEGATIVE = -1e30
LOG2E = 1.4426950408889634

SLOT_REL = (0, 1, 3, 2)
REL_SLOT = (0, 1, 3, 2)

bf16 = jnp.bfloat16
f32 = jnp.float32
VMEM = pltpu.VMEM


def cost(flops, size, exps=0):
    return pl.CostEstimate(flops=int(flops), bytes_accessed=int(size), transcendentals=int(exps))


def shifted(array, step, axis):
    size = lax.axis_size(axis)
    return lax.ppermute(array, axis, [(i, (i + step) % size) for i in range(size)])


def modulation_kernel(cond_ref, ctx_ref, shift_ref, scale_ref, gate_ref, out_ref, both, rows):
    both[...] = jnp.zeros_like(both)
    both[0:2, :] = cond_ref[...].astype(f32)
    both[2:3, :] = ctx_ref[...].astype(f32)
    raw = both[...]
    act = (raw / (1.0 + jnp.exp(-raw))).astype(bf16)
    rows[0:3, :] = jnp.dot(act, shift_ref[...], preferred_element_type=f32)[0:3]
    rows[3:6, :] = jnp.dot(act, scale_ref[...], preferred_element_type=f32)[0:3]
    rows[6:8, :] = jnp.dot(act, gate_ref[...], preferred_element_type=f32)[0:2]
    for copy in range(out_ref.shape[0]):
        out_ref[copy] = rows[...]


def modulation(copies, condition, ctx_condition, w_shift, w_scale, w_gate):
    depth, width = w_shift.shape
    return pl.pallas_call(
        modulation_kernel,
        out_shape=jax.ShapeDtypeStruct((copies, 8, width), f32),
        scratch_shapes=[VMEM((8, depth), f32), VMEM((8, width), f32)],
        cost_estimate=cost(6e6, 3 * depth * width * 2),
        name="modulation",
    )(condition, ctx_condition[None], w_shift, w_scale, w_gate)


def modulated_into(h_ref, row, x_ref, where, rows, gain, shift):
    step = 64
    for at in range(0, rows, step):
        x = x_ref[(*where, slice(at, at + step), slice(None))].astype(f32)
        mean = jnp.mean(x * x, axis=-1, keepdims=True)
        h = x * lax.rsqrt(mean + EPSILON) * gain + shift
        h_ref[row + at : row + at + step, :] = h.astype(bf16)


def turned(u, cosine, sine):
    lane = lax.broadcasted_iota(jnp.int32, u.shape, 1)
    swapped = jnp.where(lane % 64 < 32, pltpu.roll(u, 96, 1), pltpu.roll(u, 32, 1))
    return u * cosine + swapped * sine


def project_kernel(*refs):
    x_refs, refs = refs[:8], refs[8:]
    where_ref, gain_ref, mod_ref, row_cos, row_sin, col_cos, col_sin = refs[:7]
    wq_ref, wk_ref, wv_ref, q_ref, kv_ref, up_ref, down_ref, x_all, h_ref, w_all, sems = refs[7:]
    sp, tp = where_ref[0], where_ref[1]
    copies = [
        pltpu.make_async_copy(x_ref, x_all.at[i], sems.at[i]) for i, x_ref in enumerate(x_refs)
    ]
    weights = [
        pltpu.make_async_copy(wq_ref, w_all.at[:, 0:512], sems.at[8]),
        pltpu.make_async_copy(wk_ref, w_all.at[:, 512:640], sems.at[9]),
        pltpu.make_async_copy(wv_ref, w_all.at[:, 640:768], sems.at[10]),
    ]
    for copy in copies[:2] + weights + copies[2:]:
        copy.start()
    gains = [gain_ref[...] * (1.0 + mod_ref[3 + b : 4 + b, :]) for b in range(2)]
    left = lax.broadcasted_iota(jnp.int32, (GRID_W, HEAD_DIM), 1) < HEAD_DIM // 2

    def prepare(c):
        for b in range(2):
            copies[2 * c + b].wait()
            shift = mod_ref[b : b + 1, :]
            modulated_into(h_ref.at[c], b * 128, x_all, (2 * c + b,), 128, gains[b], shift)

    def table(row_ref, col_ref, row):
        parts = [
            jnp.where(left, row_ref[pl.ds(row + i, 1), :], col_ref[...]) for i in range(2)
        ]
        return jnp.concatenate(parts, axis=0)

    for c in range(4):
        prepare(c)
    for copy in weights:
        copy.wait()
    chunks = [lax.rem(tp + SLOT_REL[c], 4) for c in range(4)]
    tables = []
    for c in range(4):
        row = sp * 8 + chunks[c] * 2
        tables.append((table(row_cos, col_cos, row), table(row_sin, col_sin, row)))
    for n in range(3):
        product = jnp.dot(
            h_ref[...].reshape(1024, h_ref.shape[2]),
            w_all[:, n * 256 : n * 256 + 256],
            preferred_element_type=f32,
        )
        for c in range(4):
            tok = slice(c * 128, c * 128 + 128)
            for b in range(2):
                rows = slice(c * 256 + b * 128, c * 256 + b * 128 + 128)
                left_part = turned(product[rows, :128], *tables[c]).astype(bf16)
                if n < 2:
                    right_part = turned(product[rows, 128:], *tables[c]).astype(bf16)
                    q_ref[b, 2 * n, tok, :] = left_part
                    q_ref[b, 2 * n + 1, tok, :] = right_part
                else:
                    right_part = product[rows, 128:].astype(bf16)
                    kv_ref[b, 0, tok, :] = left_part
                    kv_ref[b, 1, tok, :] = right_part
    for c in range(4):
        tok = slice(c * 128, c * 128 + 128)
        for to_ref, edge in ((up_ref, 3), (down_ref, 0)):

            @pl.when(chunks[c] == edge)
            def _():
                to_ref[...] = kv_ref[:, :, tok, :]


def project(arrays, where, gain, mod, weights):
    width = gain.shape[1]
    anywhere = pl.BlockSpec(memory_space=pl.ANY)
    whole = pl.BlockSpec(memory_space=VMEM)
    scalars = pl.BlockSpec(memory_space=pltpu.SMEM)
    shapes = [(2, 4, 512, HEAD_DIM), (2, 2, 512, HEAD_DIM)] + [(2, 2, 128, HEAD_DIM)] * 2
    return pl.pallas_call(
        project_kernel,
        in_specs=[anywhere] * 8 + [scalars] + [whole] * 6 + [anywhere] * 3,
        out_specs=tuple(whole for _ in shapes),
        out_shape=tuple(jax.ShapeDtypeStruct(shape, bf16) for shape in shapes),
        scratch_shapes=[
            VMEM((8, 128, width), bf16),
            VMEM((4, 256, width), bf16),
            VMEM((width, 768), bf16),
            pltpu.SemaphoreType.DMA((11,)),
        ],
        cost_estimate=cost(2 * 1024 * width * 768, 8e6),
        name="project",
    )(*arrays, where, gain, mod, *rotation_tables(), *weights)


def context_kernel(x_ref, gain_ref, mod_ref, wk_ref, wv_ref, out_ref, h_ref):
    rows = x_ref.shape[1]
    gain = gain_ref[...] * (1.0 + mod_ref[5:6, :])
    shift = mod_ref[2:3, :]
    for b in range(2):
        modulated_into(h_ref, b * rows, x_ref, (b,), rows, gain, shift)
    for which, w_ref in enumerate((wk_ref, wv_ref)):
        part = jnp.dot(h_ref[...], w_ref[...], preferred_element_type=f32).astype(bf16)
        for copy in range(out_ref.shape[0]):
            for b in range(2):
                out_ref[copy, b, :, which * 128 : which * 128 + 128] = part[
                    b * rows : (b + 1) * rows
                ]


def project_context(copies, context, gain, mod, w_key, w_value):
    samples, rows, width = context.shape
    return pl.pallas_call(
        context_kernel,
        out_shape=jax.ShapeDtypeStruct((copies, samples, rows, 2 * HEAD_DIM), bf16),
        scratch_shapes=[VMEM((samples * rows, width), bf16)],
        cost_estimate=cost(2 * 2 * rows * width * 256, 2 * rows * width * 2 + width * 512),
        name="project_context",
    )(context, gain, mod, w_key, w_value)


def attention_kernel(
    where_ref, sink_ref, q_ref, kv_ref, before_ref, after_ref, ctx_ref,
    out0, out1, out2, out3, ctx_k, ctx_v, tile_k, tile_v, near_k, near_v,
):
    ctx_len = ctx_k.shape[0]
    pair = ctx_ref[:, 0].reshape(ctx_len, 2 * HEAD_DIM)
    ctx_k[...] = pair[:, :HEAD_DIM]
    ctx_v[:, :HEAD_DIM] = pair[:, HEAD_DIM:]
    ctx_v[:, HEAD_DIM:] = jnp.ones((ctx_len, HEAD_DIM), bf16)
    near_v[:, :, HEAD_DIM:] = jnp.ones((4, 384, HEAD_DIM), bf16)
    for tile, which in ((tile_k, 0), (tile_v, 1)):
        tile[0:512, :] = kv_ref[0, which]
        tile[512:640, :] = before_ref[0, which]
        tile[640:768, :] = after_ref[0, which]
    sp, tp = where_ref[0], where_ref[1]
    chunks = [lax.rem(tp + SLOT_REL[slot], 4) for slot in range(4)]
    for slot in range(4):
        prev = jnp.where(chunks[slot] == 0, 4, REL_SLOT[(SLOT_REL[slot] + 3) % 4])
        after = jnp.where(chunks[slot] == 3, 5, REL_SLOT[(SLOT_REL[slot] + 1) % 4])
        prev = pl.multiple_of(prev * 128, 128)
        after = pl.multiple_of(after * 128, 128)
        for to, start in enumerate((prev, slot * 128, after)):
            rows = slice(to * 128, to * 128 + 128)
            near_k[slot, rows, :] = tile_k[pl.ds(start, 128), :]
            near_v[slot, rows, :HEAD_DIM] = tile_v[pl.ds(start, 128), :]
    ahead = lax.broadcasted_iota(jnp.int32, (128, 128), 1) - lax.broadcasted_iota(
        jnp.int32, (128, 128), 0
    )
    factor = HEAD_DIM ** (-0.5) * LOG2E
    across = (((1,), (1,)), ((), ()))
    for slot, out_ref in enumerate((out0, out1, out2, out3)):
        q = q_ref[0, :, slot * 128 : slot * 128 + 128, :].reshape(512, HEAD_DIM)
        far = lax.dot_general(q, ctx_k[...], across, preferred_element_type=f32)
        near = lax.dot_general(q, near_k[slot], across, preferred_element_type=f32)
        no_prev = (chunks[slot] == 0) & (sp == 0)
        no_after = (chunks[slot] == 3) & (sp == SEQ // 512 - 1)
        keep_prev = ahead >= jnp.where(no_prev, 1000, 0)
        keep_after = ahead <= jnp.where(no_after, -1000, 0)
        far_weights, near_weights, sinks = [], [], []
        for n in range(4):
            rows = slice(n * 128, n * 128 + 128)
            parts = [
                far[rows],
                jnp.where(keep_prev, near[rows, :128], NEGATIVE),
                near[rows, 128:256],
                jnp.where(keep_after, near[rows, 256:], NEGATIVE),
            ]
            sink = sink_ref[n] * LOG2E
            top = functools.reduce(
                jnp.maximum, [jnp.max(part, axis=-1, keepdims=True) for part in parts]
            )
            top = jnp.maximum(top * factor, sink)
            weights = [jnp.exp2(part * factor - top).astype(bf16) for part in parts]
            far_weights.append(weights[0])
            near_weights.append(jnp.concatenate(weights[1:], axis=1))
            sinks.append(jnp.exp2(sink - top))
        both = jnp.dot(
            jnp.concatenate(far_weights, axis=0), ctx_v[...], preferred_element_type=f32
        ) + jnp.dot(
            jnp.concatenate(near_weights, axis=0), near_v[slot], preferred_element_type=f32
        )
        for n in range(4):
            rows = slice(n * 128, n * 128 + 128)
            total = both[rows, HEAD_DIM:] + sinks[n]
            out_ref[:, rows] = (both[rows, :HEAD_DIM] / total).astype(bf16)


def attention(b, where, sink, q, kv, before, after, ctx):
    parts, _, rows, _ = ctx.shape
    ctx_len = parts * rows
    work = 4 * 4 * 128 * (ctx_len + 384)
    out = pl.BlockSpec((128, 512), lambda i, *_: (0, 0))
    edge = pl.BlockSpec((1, 2, 128, HEAD_DIM), lambda i, *_: (b, 0, 0, 0))
    grid_spec = pltpu.PrefetchScalarGridSpec(
        num_scalar_prefetch=2,
        grid=(1,),
        in_specs=[
            pl.BlockSpec((1, 4, 512, HEAD_DIM), lambda i, *_: (b, 0, 0, 0)),
            pl.BlockSpec((1, 2, 512, HEAD_DIM), lambda i, *_: (b, 0, 0, 0)),
            edge, edge,
            pl.BlockSpec((parts, 1, rows, 2 * HEAD_DIM), lambda i, *_: (0, b, 0, 0)),
        ],
        out_specs=(out,) * 4,
        scratch_shapes=[
            VMEM((ctx_len, HEAD_DIM), bf16),
            VMEM((ctx_len, 2 * HEAD_DIM), bf16),
            VMEM((768, HEAD_DIM), bf16),
            VMEM((768, HEAD_DIM), bf16),
            VMEM((4, 384, HEAD_DIM), bf16),
            VMEM((4, 384, 2 * HEAD_DIM), bf16),
        ],
    )
    return pl.pallas_call(
        attention_kernel,
        grid_spec=grid_spec,
        out_shape=(jax.ShapeDtypeStruct((128, 512), bf16),) * 4,
        cost_estimate=cost(work * 512, 3e6, work),
    )(where, sink, q, kv, before, after, ctx)


def own_heads_kernel(a0_ref, a1_ref, w0_ref, branch_ref):
    heads = jnp.concatenate([a0_ref[...], a1_ref[...]], axis=0)
    part = jnp.dot(heads, w0_ref[...], preferred_element_type=f32)
    branch_ref[...] = part.astype(bf16)


def own_heads(attn, w_own):
    depth, width = w_own.shape
    tile = 1024
    whole = pl.BlockSpec((128, 512), lambda n: (0, 0))
    return pl.pallas_call(
        own_heads_kernel,
        grid=(width // tile,),
        in_specs=[whole] * 2 + [pl.BlockSpec((depth, tile), lambda n: (0, n))],
        out_specs=pl.BlockSpec((256, tile), lambda n: (0, n)),
        out_shape=jax.ShapeDtypeStruct((256, width), bf16),
        cost_estimate=cost(2 * 256 * depth * width, 3e6),
        name="own_heads",
    )(*attn, w_own)


def output_kernel(where_ref, *refs):
    a_refs, w_refs = refs[:6], refs[6:14]
    branch_ref, mod_ref, lat0_ref, lat1_ref, out_ref = refs[14:]
    low = where_ref[2] == 0
    total = branch_ref[...].astype(f32)
    pieces = (w_refs[0:2], w_refs[2:6], w_refs[6:8])
    for j in range(3):
        a = jnp.concatenate([a_refs[2 * j][...], a_refs[2 * j + 1][...]], axis=0)
        a_near = jnp.where(low, a[:, :256], a[:, 256:])
        a_far = jnp.where(low, a[:, 256:], a[:, :256])
        w = jnp.concatenate([ref[...] for ref in pieces[j]], axis=0)
        part = jnp.dot(
            jnp.concatenate([a_near, a_far], axis=1), w, preferred_element_type=f32
        )
        total = total + part.astype(bf16).astype(f32)
    for b, lat_ref in enumerate((lat0_ref, lat1_ref)):
        gate = mod_ref[6 + b : 7 + b, :]
        mixed = lat_ref[...].astype(f32) + gate * total[b * 128 : b * 128 + 128]
        out_ref[:, b, :] = mixed.astype(bf16)


def output(where, attn, gathered, branch, mod, latents):
    rows, width = latents[0].shape
    tile = 512
    whole = pl.BlockSpec((rows, 512), lambda n: (0, 0))

    def columns(*lead):
        return pl.BlockSpec((*lead, tile), lambda n: (0,) * len(lead) + (n,))

    return pl.pallas_call(
        output_kernel,
        grid=(width // tile,),
        in_specs=[pl.BlockSpec(memory_space=pltpu.SMEM)]
        + [whole] * 6
        + [columns(array.shape[0]) for array in gathered]
        + [columns(256), columns(8), columns(rows), columns(rows)],
        out_specs=columns(rows, 2),
        out_shape=jax.ShapeDtypeStruct((rows, 2, width), bf16),
        cost_estimate=cost(2 * 256 * width * width * 3 // 4, 10e6),
        name="output",
    )(where, *attn, *gathered, branch, mod, *latents)


def rotation_tables():
    quarter = HEAD_DIM // 4
    freqs = np.float32(10000.0) ** (-np.arange(quarter, dtype=np.float32) / np.float32(quarter))
    tables = []
    for count, left in ((SEQ // GRID_W, True), (GRID_W, False)):
        angle = (np.arange(count, dtype=np.float32)[:, None] * freqs).astype(np.float64)
        cosine = np.concatenate([np.cos(angle)] * 2, axis=1)
        sine = np.concatenate([-np.sin(angle), np.sin(angle)], axis=1)
        for values in (cosine, sine):
            pair = [values, np.zeros_like(values)]
            table = np.concatenate(pair if left else pair[::-1], axis=1)
            tables.append(jnp.asarray(table.astype(np.float32)))
    return tables


def block(
    latent, context, condition, ctx_condition, norm_gain, w_shift, w_scale, w_gate,
    w_query, w_key, w_value, w_out, sink,
):
    sp, tp, dp = (lax.axis_index(name) for name in ("sp", "tp", "dp"))
    n_sp, n_tp = lax.axis_size("sp"), lax.axis_size("tp")
    _, _, width = latent.shape

    own = tuple(latent[:, b] for b in range(2))
    below_0 = shifted(own[0], 1, "tp")
    above_1 = shifted(own[1], -1, "tp")
    below_1 = shifted(own[1], 1, "tp")
    above_0 = shifted(own[0], -1, "tp")
    across_0 = shifted(below_0, 1, "tp")
    across_1 = shifted(above_1, -1, "tp")

    partial = modulation(n_sp, condition, ctx_condition, w_shift, w_scale, w_gate)
    quarters = lax.all_to_all(partial, "sp", 0, 0, tiled=True)
    quarter = quarters.sum(axis=0)
    around = [quarter]
    for j in (1, 2, 3):
        around.append(shifted(quarter, -j, "tp"))
    twice = jnp.concatenate(around + around[:3], axis=1)
    mod = lax.dynamic_slice_in_dim(
        twice, (n_tp - tp) % n_tp * quarter.shape[1], width, axis=1
    )

    gain = norm_gain[None]
    ctx = project_context(n_sp, jnp.moveaxis(context, 1, 0), gain, mod, w_key, w_value)
    ctx = lax.all_to_all(ctx, "sp", 0, 0, tiled=True)

    half = lax.dynamic_slice_in_dim(w_out, dp * 256, 256, axis=0)
    w_below = shifted(half, 1, "tp")
    w_above = shifted(half, -1, "tp")
    w_across_0 = shifted(w_below[:128], 1, "tp")
    w_across_1 = shifted(w_above[128:], -1, "tp")
    gathered = []
    for array in (w_below, w_across_0, w_across_1, w_above):
        gathered.append((array, shifted(array, 1, "dp")))
    gathered = (
        *gathered[0],
        gathered[1][0], gathered[2][0], gathered[1][1], gathered[2][1],
        *gathered[3],
    )

    where = jnp.stack([sp, tp, dp]).astype(jnp.int32)
    q, kv, up, down = project(
        (*own, above_0, above_1, below_0, below_1, across_0, across_1),
        where, gain, mod, (w_query, w_key, w_value),
    )

    along = [(i, i + 1) for i in range(n_sp - 1)]
    before = lax.ppermute(up, "sp", along)
    after = lax.ppermute(down, "sp", [(j, i) for i, j in along])

    heads = [[None] * 2 for _ in range(4)]
    for b in range(2):
        attn = attention(b, where, sink, q, kv, before, after, ctx)
        heads[0][b] = attn[0]
        for j in (2, 1, 3):
            heads[j][b] = shifted(attn[REL_SLOT[j]], j, "tp")
    branch = own_heads(heads[0], w_out)
    return output(where, heads[1] + heads[2] + heads[3], gathered, branch, mod, own)


def solution(mesh):
    return jax.shard_map(
        block,
        mesh=mesh,
        in_specs=(
            P(("sp", "tp"), "dp", None),
            P("sp", "dp", None),
            P("dp", "sp"),
            P("sp"),
            P(),
            P("sp", "tp"),
            P("sp", "tp"),
            P("sp", "tp"),
            P(None, "tp"),
            P(None, "tp"),
            P(None, "tp"),
            P("tp", None),
            P("tp"),
        ),
        out_specs=P(("sp", "tp"), "dp", None),
        check_vma=False,
    )
```

profile of v0, /device:TPU:96, one launch (start us, length us, event | category | flops | bytes accessed | tf_op | source)
XLA Modules:
  0.0 157.1 jit_solution(12232392188658088015)
XLA Ops:
  0.0 3.3 %fusion = (bf16[128,1,2048]{2,1,0:T(2,128)(2,1)S(1)}, bf16[128,1,2048]{2,1,0:T(2,128)(2,1)S(1)}) fusion(bf16[128,2,2048]{2,1,0:T(2,128)(2,1)} %param.17), kind=kLoop, calls=%fused_computation.13 | loop fusion | bytes 2097152 | tf_op jit(solution)/shard_map/slice | solution.py:377
  11.4 7.0 %all-to-all-start = ((f32[16,8,512]{2,1,0:T(8,128)}), f32[16,8,512]{2,1,0:T(8,128)S(1)}, u32[]{:S(2)}, u32[]{:S(2)}) async-start(f32[16,8,512]{2,1,0:T(8,128)} %modulation.1), calls=%async_computation | async-start | bytes 524288 | tf_op jit(solution)/shard_map/all_to_all | solution.py:386
  21.4 3.3 %all-to-all-done = f32[16,8,512]{2,1,0:T(8,128)S(1)} async-done(((f32[16,8,512]{2,1,0:T(8,128)}), f32[16,8,512]{2,1,0:T(8,128)S(1)}, u32[]{:S(2)}, u32[]{:S(2)}) %all-to-all-start) | async-done | bytes 262176 | tf_op jit(solution)/shard_map/all_to_all | solution.py:386
  24.8 3.1 %collective-permute-start.6 = (f32[8,512]{1,0:T(8,128)S(1)}, f32[8,512]{1,0:T(8,128)S(1)}, u32[]{:S(2)}, u32[]{:S(2)}) collective-permute-start(f32[8,512]{1,0:T(8,128)S(1)} %reduce_sum.9), channel_id=1, source_target_pairs={{0,6},{2,0},{4,2},{6,4},{1,7},{3,1},{5,3},{7,5},{8,14},{10,8},{12,... | collective-permute-start | bytes 49160 | tf_op jit(solution)/shard_map/ppermute | solution.py:33
  27.9 2.4 %collective-permute-done.6 = f32[8,512]{1,0:T(8,128)S(1)} collective-permute-done((f32[8,512]{1,0:T(8,128)S(1)}, f32[8,512]{1,0:T(8,128)S(1)}, u32[]{:S(2)}, u32[]{:S(2)}) %collective-permute-start.6) | collective-permute-done | bytes 16416 | tf_op jit(solution)/shard_map/ppermute | solution.py:33
  30.3 2.9 %collective-permute-start.7 = (f32[8,512]{1,0:T(8,128)S(1)}, f32[8,512]{1,0:T(8,128)S(1)}, u32[]{:S(2)}, u32[]{:S(2)}) collective-permute-start(f32[8,512]{1,0:T(8,128)S(1)} %reduce_sum.9), channel_id=1, source_target_pairs={{0,4},{2,6},{4,0},{6,2},{1,5},{3,7},{5,1},{7,3},{8,12},{10,14},{12... | collective-permute-start | bytes 49160 | tf_op jit(solution)/shard_map/ppermute | solution.py:33
  33.2 2.3 %collective-permute-done.7 = f32[8,512]{1,0:T(8,128)S(1)} collective-permute-done((f32[8,512]{1,0:T(8,128)S(1)}, f32[8,512]{1,0:T(8,128)S(1)}, u32[]{:S(2)}, u32[]{:S(2)}) %collective-permute-start.7) | collective-permute-done | bytes 16416 | tf_op jit(solution)/shard_map/ppermute | solution.py:33
  37.1 3.4 %collective-permute-done.8 = f32[8,512]{1,0:T(8,128)S(1)} collective-permute-done((f32[8,512]{1,0:T(8,128)S(1)}, f32[8,512]{1,0:T(8,128)S(1)}, u32[]{:S(2)}, u32[]{:S(2)}) %collective-permute-start.8) | collective-permute-done | bytes 16416 | tf_op jit(solution)/shard_map/ppermute | solution.py:33
  41.1 2.8 %collective-permute-start.20 = (bf16[256,2048]{1,0:T(8,128)(2,1)}, bf16[256,2048]{1,0:T(8,128)(2,1)S(1)}, u32[]{:S(2)}, u32[]{:S(2)}) collective-permute-start(bf16[256,2048]{1,0:T(8,128)(2,1)} %constant_dynamic-slice_fusion), channel_id=1, source_target_pairs={{0,6},{2,0},{4,2},{6,4},{1,7},{3,1},{5,3},{7,5},{8,14},{10,8},{12,... | collective-permute-start | bytes 3145736 | tf_op jit(solution)/shard_map/ppermute | solution.py:33
  43.8 3.2 %collective-permute-start.5 = (bf16[128,2048]{1,0:T(8,128)(2,1)}, bf16[128,2048]{1,0:T(8,128)(2,1)S(1)}, u32[]{:S(2)}, u32[]{:S(2)}) collective-permute-start(bf16[128,2048]{1,0:T(8,128)(2,1)} %collective-permute-done.1.refs_3_), channel_id=1, source_target_pairs={{0,6},{2,0},{4,2},{6,4},{1,7},{3,1},{5,3},{7,5},{8,14},{10,8},{12,... | collective-permute-start | bytes 1572872 | tf_op jit(solution)/shard_map/ppermute | solution.py:33
  47.7 3.1 %project_context.1 = bf16[16,2,64,256]{3,2,1,0:T(8,128)(2,1)} custom-call(bf16[2,64,2048]{2,1,0:T(8,128)(2,1)} %bitcast.22, f32[1,2048]{1,0:T(1,128)} %bitcast.23, f32[8,2048]{1,0:T(8,128)} %constant_dynamic-slice_fusion.1.refs_10_.mod_ref.refs_15_, bf16[2048,128]{1,0:T(8,128)(2,1)} %wk_ref.1, bf16[2048,128]{1,0:T(8,128)(2,1)} %wv_ref.1), custom_call_target="tpu_custom_call" | custom-call | flops 134217728 | bytes 1572864 | tf_op jit(solution)/shard_map/project_context/pallas_call | solution.py:181
  50.8 7.0 %all-to-all-start.1 = ((bf16[16,2,64,256]{3,2,1,0:T(8,128)(2,1)}), bf16[16,2,64,256]{3,2,1,0:T(8,128)(2,1)}, u32[]{:S(2)}, u32[]{:S(2)}) async-start(bf16[16,2,64,256]{3,2,1,0:T(8,128)(2,1)} %project_context.1), calls=%async_computation.1 | async-start | bytes 2097152 | tf_op jit(solution)/shard_map/all_to_all | solution.py:398
  58.4 16.6 %collective-permute-done.4.refs_6_ = bf16[128,2048]{1,0:T(8,128)(2,1)} collective-permute-done((bf16[128,2048]{1,0:T(8,128)(2,1)}, bf16[128,2048]{1,0:T(8,128)(2,1)}, u32[]{:S(2)}, u32[]{:S(2)}) %collective-permute-start.4) | collective-permute-done | bytes 524320 | tf_op jit(solution)/shard_map/ppermute | solution.py:33
  75.8 10.0 %project.1 = (bf16[2,4,512,128]{3,2,1,0:T(8,128)(2,1)}, bf16[2,2,512,128]{3,2,1,0:T(8,128)(2,1)}, bf16[2,2,128,128]{3,2,1,0:T(8,128)(2,1)}, bf16[2,2,128,128]{3,2,1,0:T(8,128)(2,1)}) custom-call(bf16[128,2048]{1,0:T(8,128)(2,1)} %bitcast.16, bf16[128,2048]{1,0:T(8,128)(2,1)} %bitcast.20, bf16[128,2048]{1,0:T(8,128)(2,1)} %collective-permute-done.refs_2_, ...), custom_call_target="tpu_custom_call" | custom-call | flops 3221225472 | bytes 8000000 | tf_op jit(solution)/shard_map/project/pallas_call | solution.py:148
  85.8 4.5 %collective-permute-start.10 = (bf16[2,2,128,128]{3,2,1,0:T(8,128)(2,1)}, bf16[2,2,128,128]{3,2,1,0:T(8,128)(2,1)S(1)}, u32[]{:S(2)}, u32[]{:S(2)}) collective-permute-start(bf16[2,2,128,128]{3,2,1,0:T(8,128)(2,1)} %get-tuple-element.20), channel_id=1, source_target_pairs={{8,0},{16,8},{24,16},{32,24},{40,32},{48,40},{56,48},{64,56},{72,6... | collective-permute-start | bytes 393224 | tf_op jit(solution)/shard_map/ppermute | solution.py:422
  94.1 3.2 %collective-permute-start.21 = (bf16[128,2048]{1,0:T(8,128)(2,1)}, bf16[128,2048]{1,0:T(8,128)(2,1)}, u32[]{:S(2)}, u32[]{:S(2)}) collective-permute-start(bf16[128,2048]{1,0:T(8,128)(2,1)} %slice.17), channel_id=1, source_target_pairs={{0,6},{2,0},{4,2},{6,4},{1,7},{3,1},{5,3},{7,5},{8,14},{10,8},{12,... | collective-permute-start | bytes 1572872 | tf_op jit(solution)/shard_map/ppermute | solution.py:33
  100.2 7.1 %shard_map.164 = (bf16[128,512]{1,0:T(8,128)(2,1)}, bf16[128,512]{1,0:T(8,128)(2,1)}, bf16[128,512]{1,0:T(8,128)(2,1)}, bf16[128,512]{1,0:T(8,128)(2,1)}) custom-call(s32[3]{0:T(128)} %pad_add_fusion.refs_8_.where_ref, f32[4]{0:T(128)} %sink_ref.3, bf16[2,4,512,128]{3,2,1,0:T(8,128)(2,1)} %get-tuple-element.17.q_ref, ...), custom_call_target="tpu_custom_call" | custom-call | flops 1476395008 | bytes 3000000 | tf_op jit(solution)/shard_map/pallas_call | solution.py:282
  107.4 6.4 %collective-permute-done.12.refs_1_ = bf16[128,512]{1,0:T(8,128)(2,1)S(1)} collective-permute-done((bf16[128,512]{1,0:T(8,128)(2,1)}, bf16[128,512]{1,0:T(8,128)(2,1)S(1)}, u32[]{:S(2)}, u32[]{:S(2)}) %collective-permute-start.12) | collective-permute-done | bytes 131104 | tf_op jit(solution)/shard_map/ppermute | solution.py:33
  114.6 5.8 %collective-permute-done.14.refs_3_ = bf16[128,512]{1,0:T(8,128)(2,1)S(1)} collective-permute-done((bf16[128,512]{1,0:T(8,128)(2,1)}, bf16[128,512]{1,0:T(8,128)(2,1)S(1)}, u32[]{:S(2)}, u32[]{:S(2)}) %collective-permute-start.14) | collective-permute-done | bytes 131104 | tf_op jit(solution)/shard_map/ppermute | solution.py:33
  122.8 7.1 %shard_map.163 = (bf16[128,512]{1,0:T(8,128)(2,1)}, bf16[128,512]{1,0:T(8,128)(2,1)}, bf16[128,512]{1,0:T(8,128)(2,1)}, bf16[128,512]{1,0:T(8,128)(2,1)}) custom-call(s32[3]{0:T(128)} %pad_add_fusion.refs_8_.where_ref, f32[4]{0:T(128)} %sink_ref.3, bf16[2,4,512,128]{3,2,1,0:T(8,128)(2,1)} %get-tuple-element.17.q_ref, ...), custom_call_target="tpu_custom_call" | custom-call | flops 1476395008 | bytes 3000000 | tf_op jit(solution)/shard_map/pallas_call | solution.py:282
  130.2 6.7 %collective-permute-done.11.refs_0_ = bf16[128,512]{1,0:T(8,128)(2,1)S(1)} collective-permute-done((bf16[128,512]{1,0:T(8,128)(2,1)}, bf16[128,512]{1,0:T(8,128)(2,1)S(1)}, u32[]{:S(2)}, u32[]{:S(2)}) %collective-permute-start.11) | collective-permute-done | bytes 131104 | tf_op jit(solution)/shard_map/ppermute | solution.py:33
  136.9 6.7 %collective-permute-done.13.refs_2_ = bf16[128,512]{1,0:T(8,128)(2,1)S(1)} collective-permute-done((bf16[128,512]{1,0:T(8,128)(2,1)}, bf16[128,512]{1,0:T(8,128)(2,1)S(1)}, u32[]{:S(2)}, u32[]{:S(2)}) %collective-permute-start.13) | collective-permute-done | bytes 131104 | tf_op jit(solution)/shard_map/ppermute | solution.py:33
  143.6 3.1 %own_heads.1.refs_14_ = bf16[256,2048]{1,0:T(8,128)(2,1)} custom-call(bf16[128,512]{1,0:T(8,128)(2,1)} %get-tuple-element.27.a0_ref, bf16[128,512]{1,0:T(8,128)(2,1)} %get-tuple-element.28.a1_ref, bf16[512,2048]{1,0:T(8,128)(2,1)} %w0_ref.1), custom_call_target="tpu_custom_call" | custom-call | flops 536870912 | bytes 3000000 | tf_op jit(solution)/shard_map/own_heads/pallas_call | solution.py:300
  149.9 7.0 %output.1 = bf16[128,2,2048]{2,1,0:T(2,128)(2,1)} custom-call(s32[3]{0:T(128)} %pad_add_fusion.refs_8_.where_ref, bf16[128,512]{1,0:T(8,128)(2,1)} %copy-done.9, bf16[128,512]{1,0:T(8,128)(2,1)} %copy-done.6, bf16[128,512]{1,0:T(8,128)(2,1)} %copy-done.10, bf16[128,512]{1,0:T(8,128)(2,1)} %copy-done.7, bf16[128,512]{1,0:T(8,128)(2,1)} %collective-permute-done.15.refs_4_, ...), custom_call_target="tpu_custom_call" | custom-call | flops 1610612736 | bytes 10000000 | tf_op jit(solution)/shard_map/output/pallas_call | solution.py:340
  (82 shorter events, 28.5 us)
Async XLA Ops:
  3.7 37.4 %collective-permute-start.2 = (bf16[128,2048]{1,0:T(8,128)(2,1)S(1)}, bf16[128,2048]{1,0:T(8,128)(2,1)}, u32[]{:S(2)}, u32[]{:S(2)}) collective-permute-start(bf16[128,2048]{1,0:T(8,128)(2,1)S(1)} %bitcast.14), channel_id=1, source_target_pairs={{0,2},{2,4},{4,6},{6,0},{1,3},{3,5},{5,7},{7,1},{8,10},{10,12},{12... | collective-permute-start | bytes 1572872 | tf_op jit(solution)/shard_map/ppermute | solution.py:33
  5.3 38.5 %collective-permute-start = (bf16[128,2048]{1,0:T(8,128)(2,1)S(1)}, bf16[128,2048]{1,0:T(8,128)(2,1)}, u32[]{:S(2)}, u32[]{:S(2)}) collective-permute-start(bf16[128,2048]{1,0:T(8,128)(2,1)S(1)} %bitcast.15), channel_id=1, source_target_pairs={{0,6},{2,0},{4,2},{6,4},{1,7},{3,1},{5,3},{7,5},{8,14},{10,8},{12,... | collective-permute-start | bytes 1572872 | tf_op jit(solution)/shard_map/ppermute | solution.py:33
  7.3 36.5 %collective-permute-start.1 = (bf16[128,2048]{1,0:T(8,128)(2,1)S(1)}, bf16[128,2048]{1,0:T(8,128)(2,1)}, u32[]{:S(2)}, u32[]{:S(2)}) collective-permute-start(bf16[128,2048]{1,0:T(8,128)(2,1)S(1)} %bitcast.18), channel_id=1, source_target_pairs={{0,6},{2,0},{4,2},{6,4},{1,7},{3,1},{5,3},{7,5},{8,14},{10,8},{12,... | collective-permute-start | bytes 1572872 | tf_op jit(solution)/shard_map/ppermute | solution.py:33
  9.2 49.2 %collective-permute-start.3 = (bf16[128,2048]{1,0:T(8,128)(2,1)S(1)}, bf16[128,2048]{1,0:T(8,128)(2,1)}, u32[]{:S(2)}, u32[]{:S(2)}) collective-permute-start(bf16[128,2048]{1,0:T(8,128)(2,1)S(1)} %bitcast.19), channel_id=1, source_target_pairs={{0,2},{2,4},{4,6},{6,0},{1,3},{3,5},{5,7},{7,1},{8,10},{10,12},{12... | collective-permute-start | bytes 1572872 | tf_op jit(solution)/shard_map/ppermute | solution.py:33
  11.4 13.4 %all-to-all-start = ((f32[16,8,512]{2,1,0:T(8,128)}), f32[16,8,512]{2,1,0:T(8,128)S(1)}, u32[]{:S(2)}, u32[]{:S(2)}) async-start(f32[16,8,512]{2,1,0:T(8,128)} %modulation.1), calls=%async_computation | async-start | bytes 524288 | tf_op jit(solution)/shard_map/all_to_all | solution.py:386
  24.8 5.5 %collective-permute-start.6 = (f32[8,512]{1,0:T(8,128)S(1)}, f32[8,512]{1,0:T(8,128)S(1)}, u32[]{:S(2)}, u32[]{:S(2)}) collective-permute-start(f32[8,512]{1,0:T(8,128)S(1)} %reduce_sum.9), channel_id=1, source_target_pairs={{0,6},{2,0},{4,2},{6,4},{1,7},{3,1},{5,3},{7,5},{8,14},{10,8},{12,... | collective-permute-start | bytes 49160 | tf_op jit(solution)/shard_map/ppermute | solution.py:33
  40.5 51.8 %collective-permute-start.17 = (bf16[256,2048]{1,0:T(8,128)(2,1)}, bf16[256,2048]{1,0:T(8,128)(2,1)S(1)}, u32[]{:S(2)}, u32[]{:S(2)}) collective-permute-start(bf16[256,2048]{1,0:T(8,128)(2,1)} %constant_dynamic-slice_fusion), channel_id=1, source_target_pairs={{0,2},{2,4},{4,6},{6,0},{1,3},{3,5},{5,7},{7,1},{8,10},{10,12},{12... | collective-permute-start | bytes 3145736 | tf_op jit(solution)/shard_map/ppermute | solution.py:33
  41.1 52.2 %collective-permute-start.20 = (bf16[256,2048]{1,0:T(8,128)(2,1)}, bf16[256,2048]{1,0:T(8,128)(2,1)S(1)}, u32[]{:S(2)}, u32[]{:S(2)}) collective-permute-start(bf16[256,2048]{1,0:T(8,128)(2,1)} %constant_dynamic-slice_fusion), channel_id=1, source_target_pairs={{0,6},{2,0},{4,2},{6,4},{1,7},{3,1},{5,3},{7,5},{8,14},{10,8},{12,... | collective-permute-start | bytes 3145736 | tf_op jit(solution)/shard_map/ppermute | solution.py:33
  43.8 31.2 %collective-permute-start.4 = (bf16[128,2048]{1,0:T(8,128)(2,1)}, bf16[128,2048]{1,0:T(8,128)(2,1)}, u32[]{:S(2)}, u32[]{:S(2)}) collective-permute-start(bf16[128,2048]{1,0:T(8,128)(2,1)} %collective-permute-done.2.refs_4_), channel_id=1, source_target_pairs={{0,2},{2,4},{4,6},{6,0},{1,3},{3,5},{5,7},{7,1},{8,10},{10,12},{12... | collective-permute-start | bytes 1572872 | tf_op jit(solution)/shard_map/ppermute | solution.py:33
  43.8 31.2 %collective-permute-start.5 = (bf16[128,2048]{1,0:T(8,128)(2,1)}, bf16[128,2048]{1,0:T(8,128)(2,1)S(1)}, u32[]{:S(2)}, u32[]{:S(2)}) collective-permute-start(bf16[128,2048]{1,0:T(8,128)(2,1)} %collective-permute-done.1.refs_3_), channel_id=1, source_target_pairs={{0,6},{2,0},{4,2},{6,4},{1,7},{3,1},{5,3},{7,5},{8,14},{10,8},{12,... | collective-permute-start | bytes 1572872 | tf_op jit(solution)/shard_map/ppermute | solution.py:33
  50.8 48.7 %all-to-all-start.1 = ((bf16[16,2,64,256]{3,2,1,0:T(8,128)(2,1)}), bf16[16,2,64,256]{3,2,1,0:T(8,128)(2,1)}, u32[]{:S(2)}, u32[]{:S(2)}) async-start(bf16[16,2,64,256]{3,2,1,0:T(8,128)(2,1)} %project_context.1), calls=%async_computation.1 | async-start | bytes 2097152 | tf_op jit(solution)/shard_map/all_to_all | solution.py:398
  85.8 11.5 %collective-permute-start.10 = (bf16[2,2,128,128]{3,2,1,0:T(8,128)(2,1)}, bf16[2,2,128,128]{3,2,1,0:T(8,128)(2,1)S(1)}, u32[]{:S(2)}, u32[]{:S(2)}) collective-permute-start(bf16[2,2,128,128]{3,2,1,0:T(8,128)(2,1)} %get-tuple-element.20), channel_id=1, source_target_pairs={{8,0},{16,8},{24,16},{32,24},{40,32},{48,40},{56,48},{64,56},{72,6... | collective-permute-start | bytes 393224 | tf_op jit(solution)/shard_map/ppermute | solution.py:422
  90.3 9.2 %collective-permute-start.9 = (bf16[2,2,128,128]{3,2,1,0:T(8,128)(2,1)}, bf16[2,2,128,128]{3,2,1,0:T(8,128)(2,1)S(1)}, u32[]{:S(2)}, u32[]{:S(2)}) collective-permute-start(bf16[2,2,128,128]{3,2,1,0:T(8,128)(2,1)} %get-tuple-element.19), channel_id=1, source_target_pairs={{0,8},{8,16},{16,24},{24,32},{32,40},{40,48},{48,56},{56,64},{64,7... | collective-permute-start | bytes 393224 | tf_op jit(solution)/shard_map/ppermute | solution.py:421
  93.2 29.1 %collective-permute-start.19 = (bf16[128,2048]{1,0:T(8,128)(2,1)}, bf16[128,2048]{1,0:T(8,128)(2,1)}, u32[]{:S(2)}, u32[]{:S(2)}) collective-permute-start(bf16[128,2048]{1,0:T(8,128)(2,1)} %slice.16), channel_id=1, source_target_pairs={{0,2},{2,4},{4,6},{6,0},{1,3},{3,5},{5,7},{7,1},{8,10},{10,12},{12... | collective-permute-start | bytes 1572872 | tf_op jit(solution)/shard_map/ppermute | solution.py:33
  94.1 28.2 %collective-permute-start.21 = (bf16[128,2048]{1,0:T(8,128)(2,1)}, bf16[128,2048]{1,0:T(8,128)(2,1)}, u32[]{:S(2)}, u32[]{:S(2)}) collective-permute-start(bf16[128,2048]{1,0:T(8,128)(2,1)} %slice.17), channel_id=1, source_target_pairs={{0,6},{2,0},{4,2},{6,4},{1,7},{3,1},{5,3},{7,5},{8,14},{10,8},{12,... | collective-permute-start | bytes 1572872 | tf_op jit(solution)/shard_map/ppermute | solution.py:33
  97.4 51.6 %collective-permute-start.18 = (bf16[256,2048]{1,0:T(8,128)(2,1)S(1)}, bf16[256,2048]{1,0:T(8,128)(2,1)S(1)}, u32[]{:S(2)}, u32[]{:S(2)}) collective-permute-start(bf16[256,2048]{1,0:T(8,128)(2,1)S(1)} %collective-permute-done.17.refs_6_), channel_id=1, source_target_pairs={{0,1},{1,0},{2,3},{3,2},{4,5},{5,4},{6,7},{7,6},{8,9},{9,8},{10,11... | collective-permute-start | bytes 3145736 | tf_op jit(solution)/shard_map/ppermute | solution.py:33
  97.4 51.6 %collective-permute-start.24 = (bf16[256,2048]{1,0:T(8,128)(2,1)S(1)}, bf16[256,2048]{1,0:T(8,128)(2,1)}, u32[]{:S(2)}, u32[]{:S(2)}) collective-permute-start(bf16[256,2048]{1,0:T(8,128)(2,1)S(1)} %collective-permute-done.20.refs_12_), channel_id=1, source_target_pairs={{0,1},{1,0},{2,3},{3,2},{4,5},{5,4},{6,7},{7,6},{8,9},{9,8},{10,11... | collective-permute-start | bytes 3145736 | tf_op jit(solution)/shard_map/ppermute | solution.py:33
  107.3 6.5 %collective-permute-start.12 = (bf16[128,512]{1,0:T(8,128)(2,1)}, bf16[128,512]{1,0:T(8,128)(2,1)S(1)}, u32[]{:S(2)}, u32[]{:S(2)}) collective-permute-start(bf16[128,512]{1,0:T(8,128)(2,1)} %get-tuple-element.22), channel_id=1, source_target_pairs={{0,2},{2,4},{4,6},{6,0},{1,3},{3,5},{5,7},{7,1},{8,10},{10,12},{12... | collective-permute-start | bytes 393224 | tf_op jit(solution)/shard_map/ppermute | solution.py:33
  113.8 6.7 %collective-permute-start.14 = (bf16[128,512]{1,0:T(8,128)(2,1)}, bf16[128,512]{1,0:T(8,128)(2,1)S(1)}, u32[]{:S(2)}, u32[]{:S(2)}) collective-permute-start(bf16[128,512]{1,0:T(8,128)(2,1)} %get-tuple-element.24), channel_id=1, source_target_pairs={{0,4},{2,6},{4,0},{6,2},{1,5},{3,7},{5,1},{7,3},{8,12},{10,14},{12... | collective-permute-start | bytes 393224 | tf_op jit(solution)/shard_map/ppermute | solution.py:33
  120.5 9.5 %collective-permute-start.16 = (bf16[128,512]{1,0:T(8,128)(2,1)}, bf16[128,512]{1,0:T(8,128)(2,1)S(1)}, u32[]{:S(2)}, u32[]{:S(2)}) collective-permute-start(bf16[128,512]{1,0:T(8,128)(2,1)} %get-tuple-element.26), channel_id=1, source_target_pairs={{0,6},{2,0},{4,2},{6,4},{1,7},{3,1},{5,3},{7,5},{8,14},{10,8},{12,... | collective-permute-start | bytes 393224 | tf_op jit(solution)/shard_map/ppermute | solution.py:33
  122.3 26.6 %collective-permute-start.22 = (bf16[128,2048]{1,0:T(8,128)(2,1)}, bf16[128,2048]{1,0:T(8,128)(2,1)}, u32[]{:S(2)}, u32[]{:S(2)}) collective-permute-start(bf16[128,2048]{1,0:T(8,128)(2,1)} %collective-permute-done.19.refs_8_), channel_id=1, source_target_pairs={{0,1},{1,0},{2,3},{3,2},{4,5},{5,4},{6,7},{7,6},{8,9},{9,8},{10,11... | collective-permute-start | bytes 1572872 | tf_op jit(solution)/shard_map/ppermute | solution.py:33
  122.3 26.6 %collective-permute-start.23 = (bf16[128,2048]{1,0:T(8,128)(2,1)}, bf16[128,2048]{1,0:T(8,128)(2,1)}, u32[]{:S(2)}, u32[]{:S(2)}) collective-permute-start(bf16[128,2048]{1,0:T(8,128)(2,1)} %collective-permute-done.21.refs_9_), channel_id=1, source_target_pairs={{0,1},{1,0},{2,3},{3,2},{4,5},{5,4},{6,7},{7,6},{8,9},{9,8},{10,11... | collective-permute-start | bytes 1572872 | tf_op jit(solution)/shard_map/ppermute | solution.py:33
  130.0 7.0 %collective-permute-start.11 = (bf16[128,512]{1,0:T(8,128)(2,1)}, bf16[128,512]{1,0:T(8,128)(2,1)S(1)}, u32[]{:S(2)}, u32[]{:S(2)}) collective-permute-start(bf16[128,512]{1,0:T(8,128)(2,1)} %get-tuple-element.21), channel_id=1, source_target_pairs={{0,2},{2,4},{4,6},{6,0},{1,3},{3,5},{5,7},{7,1},{8,10},{10,12},{12... | collective-permute-start | bytes 393224 | tf_op jit(solution)/shard_map/ppermute | solution.py:33
  136.9 6.7 %collective-permute-start.13 = (bf16[128,512]{1,0:T(8,128)(2,1)}, bf16[128,512]{1,0:T(8,128)(2,1)S(1)}, u32[]{:S(2)}, u32[]{:S(2)}) collective-permute-start(bf16[128,512]{1,0:T(8,128)(2,1)} %get-tuple-element.23), channel_id=1, source_target_pairs={{0,4},{2,6},{4,0},{6,2},{1,5},{3,7},{5,1},{7,3},{8,12},{10,14},{12... | collective-permute-start | bytes 393224 | tf_op jit(solution)/shard_map/ppermute | solution.py:33
  (17 other events, 159.9 us)
where the time goes:
time: 158 us; the launch traced here: 157 us
  waiting for transfers between devices  57.6 us (36%)
  starting transfers between devices  47.2 us (30%)
  Pallas kernels  39.4 us (25%)
  local copies, waits for them, and re-layouts  11.9 us (8%)
    ppermute x23, waiting for transfers between devices, shifted(): lax.ppermute(array, axis, [(i, (i + step) % size) for i in range(size)])  52.6 us
    ppermute x23, starting transfers between devices, shifted(): lax.ppermute(array, axis, [(i, (i + step) % size) for i in range(size)])  26.8 us
    pallas_call x2, Pallas kernels, attention(): pl.pallas_call(attention_kernel, grid_spec=grid_spec, out_shape=(jax.Shap...  14.3 us
    pallas_call x1, Pallas kernels, project(): pl.pallas_call(project_kernel, in_specs=[anywhere] * 8 + [scalars] + [who...  10 us
    all_to_all x1, starting transfers between devices, block(): quarters = lax.all_to_all(partial, 'sp', 0, 0, tiled=True)  6.99 us
    all_to_all x1, starting transfers between devices, block(): ctx = lax.all_to_all(ctx, 'sp', 0, 0, tiled=True)  6.99 us
    pallas_call x1, Pallas kernels, output(): pl.pallas_call(output_kernel, grid=(width // tile,), in_specs=[pl.BlockSp...  6.96 us
    unnamed x37, local copies, waits for them, and re-layouts  5.05 us
  transfers between devices with their start and end apart: 27, of which 11 were waited for; matrix products, arithmetic and copies ran while one was open for 4% of the time, Pallas kernels for 21%

commit v1 on v0

v1 whole, which is shorter than its diff:
```python
import functools

import jax
import jax.numpy as jnp
import numpy as np
from jax import lax
from jax.experimental import pallas as pl
from jax.experimental.pallas import tpu as pltpu
from jax.sharding import PartitionSpec as P


HEAD_DIM = 128
GRID_W = 64
SEQ = 8192
EPSILON = 1e-06
NEGATIVE = -1e30
LOG2E = 1.4426950408889634

SLOT_REL = (0, 1, 3, 2)
REL_SLOT = (0, 1, 3, 2)

bf16 = jnp.bfloat16
f32 = jnp.float32
VMEM = pltpu.VMEM


def cost(flops, size, exps=0):
    return pl.CostEstimate(flops=int(flops), bytes_accessed=int(size), transcendentals=int(exps))


def shifted(array, step, axis):
    size = lax.axis_size(axis)
    return lax.ppermute(array, axis, [(i, (i + step) % size) for i in range(size)])


def modulation_kernel(cond_ref, ctx_ref, shift_ref, scale_ref, gate_ref, out_ref, both, rows):
    both[...] = jnp.zeros_like(both)
    both[0:2, :] = cond_ref[...].astype(f32)
    both[2:3, :] = ctx_ref[...].astype(f32)
    raw = both[...]
    act = (raw / (1.0 + jnp.exp(-raw))).astype(bf16)
    rows[0:3, :] = jnp.dot(act, shift_ref[...], preferred_element_type=f32)[0:3]
    rows[3:6, :] = jnp.dot(act, scale_ref[...], preferred_element_type=f32)[0:3]
    rows[6:8, :] = jnp.dot(act, gate_ref[...], preferred_element_type=f32)[0:2]
    for copy in range(out_ref.shape[0]):
        out_ref[copy] = rows[...]


def modulation(copies, condition, ctx_condition, w_shift, w_scale, w_gate):
    depth, width = w_shift.shape
    return pl.pallas_call(
        modulation_kernel,
        out_shape=jax.ShapeDtypeStruct((copies, 8, width), f32),
        scratch_shapes=[VMEM((8, depth), f32), VMEM((8, width), f32)],
        cost_estimate=cost(6e6, 3 * depth * width * 2),
        name="modulation",
        compiler_params=pltpu.CompilerParams(vmem_limit_bytes=4 << 20),
    )(condition, ctx_condition[None], w_shift, w_scale, w_gate)


def modulated_into(h_ref, row, x_ref, where, rows, gain, shift):
    step = 64
    for at in range(0, rows, step):
        x = x_ref[(*where, slice(at, at + step), slice(None))].astype(f32)
        mean = jnp.mean(x * x, axis=-1, keepdims=True)
        h = x * lax.rsqrt(mean + EPSILON) * gain + shift
        h_ref[row + at : row + at + step, :] = h.astype(bf16)


def turned(u, cosine, sine):
    lane = lax.broadcasted_iota(jnp.int32, u.shape, 1)
    swapped = jnp.where(lane % 64 < 32, pltpu.roll(u, 96, 1), pltpu.roll(u, 32, 1))
    return u * cosine + swapped * sine


def project_kernel(*refs):
    x_refs, refs = refs[:8], refs[8:]
    where_ref, gain_ref, mod_ref, row_cos, row_sin, col_cos, col_sin = refs[:7]
    wq_ref, wk_ref, wv_ref, q_ref, kv_ref, up_ref, down_ref, h_ref, w_kv = refs[7:]
    sp, tp = where_ref[0], where_ref[1]
    gains = [gain_ref[...] * (1.0 + mod_ref[3 + b : 4 + b, :]) for b in range(2)]
    left = lax.broadcasted_iota(jnp.int32, (GRID_W, HEAD_DIM), 1) < HEAD_DIM // 2

    def prepare(c):
        for b in range(2):
            shift = mod_ref[b : b + 1, :]
            modulated_into(h_ref.at[c], b * 128, x_refs[2 * c + b], (), 128, gains[b], shift)

    def table(row_ref, col_ref, row):
        parts = [
            jnp.where(left, row_ref[pl.ds(row + i, 1), :], col_ref[...]) for i in range(2)
        ]
        return jnp.concatenate(parts, axis=0)

    for c in range(4):
        prepare(c)
    w_kv[:, :HEAD_DIM] = wk_ref[...]
    w_kv[:, HEAD_DIM:] = wv_ref[...]
    chunks = [lax.rem(tp + SLOT_REL[c], 4) for c in range(4)]
    tables = []
    for c in range(4):
        row = sp * 8 + chunks[c] * 2
        tables.append((table(row_cos, col_cos, row), table(row_sin, col_sin, row)))
    for n in range(3):
        product = jnp.dot(
            h_ref[...].reshape(1024, h_ref.shape[2]),
            wq_ref[:, n * 256 : n * 256 + 256] if n < 2 else w_kv[...],
            preferred_element_type=f32,
        )
        for c in range(4):
            tok = slice(c * 128, c * 128 + 128)
            for b in range(2):
                rows = slice(c * 256 + b * 128, c * 256 + b * 128 + 128)
                left_part = turned(product[rows, :128], *tables[c]).astype(bf16)
                if n < 2:
                    right_part = turned(product[rows, 128:], *tables[c]).astype(bf16)
                    q_ref[b, 2 * n, tok, :] = left_part
                    q_ref[b, 2 * n + 1, tok, :] = right_part
                else:
                    right_part = product[rows, 128:].astype(bf16)
                    kv_ref[b, 0, tok, :] = left_part
                    kv_ref[b, 1, tok, :] = right_part
    for c in range(4):
        tok = slice(c * 128, c * 128 + 128)
        for to_ref, edge in ((up_ref, 3), (down_ref, 0)):

            @pl.when(chunks[c] == edge)
            def _():
                to_ref[...] = kv_ref[:, :, tok, :]


def project(arrays, where, gain, mod, weights):
    width = gain.shape[1]
    whole = pl.BlockSpec(memory_space=VMEM)
    scalars = pl.BlockSpec(memory_space=pltpu.SMEM)
    shapes = [(2, 4, 512, HEAD_DIM), (2, 2, 512, HEAD_DIM)] + [(2, 2, 128, HEAD_DIM)] * 2
    return pl.pallas_call(
        project_kernel,
        in_specs=[whole] * 8 + [scalars] + [whole] * 9,
        out_specs=tuple(whole for _ in shapes),
        out_shape=tuple(jax.ShapeDtypeStruct(shape, bf16) for shape in shapes),
        scratch_shapes=[
            VMEM((4, 256, width), bf16),
            VMEM((width, 2 * HEAD_DIM), bf16),
        ],
        cost_estimate=cost(2 * 1024 * width * 768, 8e6),
        name="project",
        compiler_params=pltpu.CompilerParams(vmem_limit_bytes=28 << 20),
    )(*arrays, where, gain, mod, *rotation_tables(), *weights)


def context_kernel(
    x_ref, where_ref, gain_ref, m0_ref, m1_ref, m2_ref, m3_ref, wk_ref, wv_ref,
    out_ref, mod_ref, h_ref,
):
    rows = x_ref.shape[1]
    quarter = m0_ref.shape[1]
    for j, m_ref in enumerate((m0_ref, m1_ref, m2_ref, m3_ref)):
        at = pl.multiple_of(lax.rem(where_ref[1] + j, 4) * quarter, quarter)
        mod_ref[:, pl.ds(at, quarter)] = m_ref[...]
    gain = gain_ref[...] * (1.0 + mod_ref[5:6, :])
    shift = mod_ref[2:3, :]
    for b in range(2):
        modulated_into(h_ref, b * rows, x_ref, (b,), rows, gain, shift)
    for which, w_ref in enumerate((wk_ref, wv_ref)):
        part = jnp.dot(h_ref[...], w_ref[...], preferred_element_type=f32).astype(bf16)
        for copy in range(out_ref.shape[0]):
            for b in range(2):
                out_ref[copy, b, :, which * 128 : which * 128 + 128] = part[
                    b * rows : (b + 1) * rows
                ]


def project_context(copies, context, where, gain, quarters, w_key, w_value):
    samples, rows, width = context.shape
    return pl.pallas_call(
        context_kernel,
        in_specs=[pl.BlockSpec(memory_space=VMEM), pl.BlockSpec(memory_space=pltpu.SMEM)]
        + [pl.BlockSpec(memory_space=VMEM)] * 7,
        out_shape=(
            jax.ShapeDtypeStruct((copies, samples, rows, 2 * HEAD_DIM), bf16),
            jax.ShapeDtypeStruct((8, width), f32),
        ),
        scratch_shapes=[VMEM((samples * rows, width), bf16)],
        cost_estimate=cost(2 * 2 * rows * width * 256, 2 * rows * width * 2 + width * 512),
        name="project_context",
        compiler_params=pltpu.CompilerParams(vmem_limit_bytes=10 << 20),
    )(context, where, gain, *quarters, w_key, w_value)


def attention_kernel(
    slots, where_ref, sink_ref, q_ref, kv_ref, before_ref, after_ref, ctx_ref, *refs
):
    if slots == (0,):
        w_ref, branch_ref, heads = refs[0], refs[1], refs[-1]
        outs, refs = (heads,), refs[2:-1]
    else:
        outs, refs = refs[: len(slots)], refs[len(slots) :]
    ctx_v, tile_k, tile_v, near_k, near_v = refs
    ctx_len = ctx_v.shape[0]
    sp, tp = where_ref[0], where_ref[1]
    ahead = lax.broadcasted_iota(jnp.int32, (128, 128), 1) - lax.broadcasted_iota(
        jnp.int32, (128, 128), 0
    )
    factor = HEAD_DIM ** (-0.5) * LOG2E
    across = (((1,), (1,)), ((), ()))
    ctx_v[:, HEAD_DIM:] = jnp.ones((ctx_len, HEAD_DIM), bf16)
    near_v[:, :, HEAD_DIM:] = jnp.ones((len(slots), 384, HEAD_DIM), bf16)
    for b in range(2):
        ctx_k = ctx_ref[:, b, :, :HEAD_DIM].reshape(ctx_len, HEAD_DIM)
        ctx_v[:, :HEAD_DIM] = ctx_ref[:, b, :, HEAD_DIM:].reshape(ctx_len, HEAD_DIM)
        for tile, which in ((tile_k, 0), (tile_v, 1)):
            tile[0:512, :] = kv_ref[b, which]
            tile[512:640, :] = before_ref[b, which]
            tile[640:768, :] = after_ref[b, which]
        for at, (slot, out_ref) in enumerate(zip(slots, outs)):
            chunk = lax.rem(tp + SLOT_REL[slot], 4)
            prev = jnp.where(chunk == 0, 4, REL_SLOT[(SLOT_REL[slot] + 3) % 4])
            after = jnp.where(chunk == 3, 5, REL_SLOT[(SLOT_REL[slot] + 1) % 4])
            starts = (pl.multiple_of(prev * 128, 128), slot * 128, pl.multiple_of(after * 128, 128))
            for to, start in enumerate(starts):
                rows = slice(to * 128, to * 128 + 128)
                near_k[at, rows, :] = tile_k[pl.ds(start, 128), :]
                near_v[at, rows, :HEAD_DIM] = tile_v[pl.ds(start, 128), :]
            q = q_ref[b, :, slot * 128 : slot * 128 + 128, :].reshape(512, HEAD_DIM)
            far = lax.dot_general(q, ctx_k, across, preferred_element_type=f32)
            near = lax.dot_general(q, near_k[at], across, preferred_element_type=f32)
            no_prev = (chunk == 0) & (sp == 0)
            no_after = (chunk == 3) & (sp == SEQ // 512 - 1)
            keep_prev = ahead >= jnp.where(no_prev, 1000, 0)
            keep_after = ahead <= jnp.where(no_after, -1000, 0)
            far_weights, near_weights, sinks = [], [], []
            for n in range(4):
                rows = slice(n * 128, n * 128 + 128)
                parts = [
                    far[rows],
                    jnp.where(keep_prev, near[rows, :128], NEGATIVE),
                    near[rows, 128:256],
                    jnp.where(keep_after, near[rows, 256:], NEGATIVE),
                ]
                sink = sink_ref[n] * LOG2E
                top = functools.reduce(
                    jnp.maximum, [jnp.max(part, axis=-1, keepdims=True) for part in parts]
                )
                top = jnp.maximum(top * factor, sink)
                weights = [jnp.exp2(part * factor - top).astype(bf16) for part in parts]
                far_weights.append(weights[0])
                near_weights.append(jnp.concatenate(weights[1:], axis=1))
                sinks.append(jnp.exp2(sink - top))
            both = jnp.dot(
                jnp.concatenate(far_weights, axis=0), ctx_v[...], preferred_element_type=f32
            ) + jnp.dot(
                jnp.concatenate(near_weights, axis=0), near_v[at], preferred_element_type=f32
            )
            for n in range(4):
                rows = slice(n * 128, n * 128 + 128)
                total = both[rows, HEAD_DIM:] + sinks[n]
                out_ref[b * 128 : b * 128 + 128, rows] = (
                    both[rows, :HEAD_DIM] / total
                ).astype(bf16)
    if slots == (0,):
        part = jnp.dot(heads[...], w_ref[...], preferred_element_type=f32)
        branch_ref[...] = part.astype(bf16)


def attention(slots, where, sink, q, kv, before, after, ctx, w_own=None):
    parts, _, rows, _ = ctx.shape
    ctx_len = parts * rows
    work = 2 * len(slots) * 4 * 128 * (ctx_len + 384)
    whole = pl.BlockSpec(memory_space=VMEM)
    scalars = pl.BlockSpec(memory_space=pltpu.SMEM)
    operands = [where, sink, q, kv, before, after, ctx]
    in_specs = [scalars] * 2 + [whole] * 5
    scratch = [
        VMEM((ctx_len, 2 * HEAD_DIM), bf16),
        VMEM((768, HEAD_DIM), bf16),
        VMEM((768, HEAD_DIM), bf16),
        VMEM((len(slots), 384, HEAD_DIM), bf16),
        VMEM((len(slots), 384, 2 * HEAD_DIM), bf16),
    ]
    shapes = [(256, 512)] * len(slots)
    if slots == (0,):
        operands.append(w_own)
        in_specs.append(whole)
        shapes = [(256, w_own.shape[1])]
        scratch.append(VMEM((256, 512), bf16))
    return pl.pallas_call(
        functools.partial(attention_kernel, slots),
        in_specs=in_specs,
        out_specs=tuple(whole for _ in shapes),
        out_shape=tuple(jax.ShapeDtypeStruct(shape, bf16) for shape in shapes),
        scratch_shapes=scratch,
        cost_estimate=cost(work * 512, 4e6, work),
        compiler_params=pltpu.CompilerParams(vmem_limit_bytes=24 << 20),
    )(*operands)


def output_kernel(where_ref, *refs):
    a_refs, w_refs = refs[:3], refs[3:11]
    branch_ref, mod_ref, lat0_ref, lat1_ref, out_ref = refs[11:]
    sp, dp = where_ref[0], where_ref[2]
    odd_x, odd_z = lax.rem(sp, 2), lax.rem(lax.div(sp, 4), 2)
    at_two = []
    for core, odd in ((dp, jnp.where(dp == 0, odd_x, odd_z)), (1 - dp, jnp.where(dp == 0, odd_z, odd_x))):
        at_two += [core * 256 + odd * 128, core * 256 + (1 - odd) * 128]
    groups = (
        (a_refs[0], (2, 6), (dp * 256, 256 - dp * 256)),
        (a_refs[1], (0, 1, 4, 5), at_two),
        (a_refs[2], (3, 7), (dp * 256, 256 - dp * 256)),
    )
    heads = []
    for a_ref, pieces, starts in groups:
        parts = [
            a_ref[:, pl.ds(pl.multiple_of(start, 128), w_refs[i].shape[0])]
            for i, start in zip(pieces, starts)
        ]
        heads.append(jnp.concatenate(parts, axis=1))
    tile = 512
    for n in range(0, out_ref.shape[2], tile):
        cols = slice(n, n + tile)
        total = branch_ref[:, cols].astype(f32)
        for a, (_, pieces, _) in zip(heads, groups):
            w = jnp.concatenate([w_refs[i][:, cols] for i in pieces], axis=0)
            part = jnp.dot(a, w, preferred_element_type=f32)
            total = total + part.astype(bf16).astype(f32)
        for b, lat_ref in enumerate((lat0_ref, lat1_ref)):
            gate = mod_ref[6 + b : 7 + b, cols]
            mixed = lat_ref[:, cols].astype(f32) + gate * total[b * 128 : b * 128 + 128]
            out_ref[:, b, cols] = mixed.astype(bf16)


def output(where, attn, gathered, branch, mod, latents):
    rows, width = latents[0].shape
    whole = pl.BlockSpec(memory_space=VMEM)
    return pl.pallas_call(
        output_kernel,
        in_specs=[pl.BlockSpec(memory_space=pltpu.SMEM)] + [whole] * (len(attn) + len(gathered) + 4),
        out_specs=whole,
        out_shape=jax.ShapeDtypeStruct((rows, 2, width), bf16),
        cost_estimate=cost(2 * 256 * width * width * 3 // 4, 10e6),
        name="output",
        compiler_params=pltpu.CompilerParams(vmem_limit_bytes=22 << 20),
    )(where, *attn, *gathered, branch, mod, *latents)


def rotation_tables():
    quarter = HEAD_DIM // 4
    freqs = np.float32(10000.0) ** (-np.arange(quarter, dtype=np.float32) / np.float32(quarter))
    tables = []
    for count, left in ((SEQ // GRID_W, True), (GRID_W, False)):
        angle = (np.arange(count, dtype=np.float32)[:, None] * freqs).astype(np.float64)
        cosine = np.concatenate([np.cos(angle)] * 2, axis=1)
        sine = np.concatenate([-np.sin(angle), np.sin(angle)], axis=1)
        for values in (cosine, sine):
            pair = [values, np.zeros_like(values)]
            table = np.concatenate(pair if left else pair[::-1], axis=1)
            tables.append(jnp.asarray(table.astype(np.float32)))
    return tables


def block(
    latent, context, condition, ctx_condition, norm_gain, w_shift, w_scale, w_gate,
    w_query, w_key, w_value, w_out, sink,
):
    sp, tp, dp = (lax.axis_index(name) for name in ("sp", "tp", "dp"))
    n_sp = lax.axis_size("sp")
    where = jnp.stack([sp, tp, dp]).astype(jnp.int32)

    own = tuple(latent[:, b] for b in range(2))
    below_0 = shifted(own[0], 1, "tp")
    above_1 = shifted(own[1], -1, "tp")
    below_1 = shifted(own[1], 1, "tp")
    above_0 = shifted(own[0], -1, "tp")
    across_0 = shifted(below_0, 1, "tp")
    across_1 = shifted(above_1, -1, "tp")

    partial = modulation(n_sp, condition, ctx_condition, w_shift, w_scale, w_gate)
    quarters = lax.all_to_all(partial, "sp", 0, 0, tiled=True)
    quarter = quarters.sum(axis=0)
    around = [quarter]
    for j in (1, 2, 3):
        around.append(shifted(quarter, -j, "tp"))
    gain = norm_gain[None]
    ctx, mod = project_context(
        n_sp, jnp.moveaxis(context, 1, 0), where, gain, around, w_key, w_value
    )
    ctx = lax.all_to_all(ctx, "sp", 0, 0, tiled=True)

    half = lax.dynamic_slice_in_dim(w_out, dp * 256, 256, axis=0)
    parity = jnp.where(dp == 0, sp % 2, sp // 4 % 2)
    part = lax.dynamic_slice_in_dim(w_out, dp * 256 + parity * 128, 128, axis=0)
    pairs = []
    for s in range(n_sp):
        for d in range(2):
            pairs.append((s * 2 + d, (s ^ (1 if d == 0 else 4)) * 2 + d))
    mine = shifted(part, 2, "tp")
    theirs = lax.ppermute(mine, ("sp", "dp"), pairs)
    below = shifted(half, 1, "tp")
    above = shifted(half, -1, "tp")
    gathered = [mine, theirs, below, above]
    for array in tuple(gathered):
        gathered.append(shifted(array, 1, "dp"))

    q, kv, up, down = project(
        (*own, above_0, above_1, below_0, below_1, across_0, across_1),
        where, gain, mod, (w_query, w_key, w_value),
    )

    along = [(i, i + 1) for i in range(n_sp - 1)]
    before = lax.ppermute(up, "sp", along)
    after = lax.ppermute(down, "sp", [(j, i) for i, j in along])

    attn = attention((3, 1, 2), where, sink, q, kv, before, after, ctx)
    heads = []
    for j, array in ((1, attn[1]), (2, attn[0]), (3, attn[2])):
        heads.append(shifted(array, j, "tp"))
    (branch,) = attention((0,), where, sink, q, kv, before, after, ctx, w_out)
    return output(where, heads, gathered, branch, mod, own)


def solution(mesh):
    return jax.shard_map(
        block,
        mesh=mesh,
        in_specs=(
            P(("sp", "tp"), "dp", None),
            P("sp", "dp", None),
            P("dp", "sp"),
            P("sp"),
            P(),
            P("sp", "tp"),
            P("sp", "tp"),
            P("sp", "tp"),
            P(None, "tp"),
            P(None, "tp"),
            P(None, "tp"),
            P("tp", None),
            P("tp"),
        ),
        out_specs=P(("sp", "tp"), "dp", None),
        check_vma=False,
    )
```

time: 158 us -> 153 us (0.968)
  the two profiles are of different devices: /device:TPU:96 before, /device:TPU:32 now
where the time goes in v1:
time: 153 us
  waiting for transfers between devices  56.3 us (37%)
  starting transfers between devices  35.2 us (23%)
  Pallas kernels  26.2 us (17%)
  local copies, waits for them, and re-layouts  19.9 us (13%)
  blocking collectives  14.5 us (9%)
    ppermute x19, waiting for transfers between devices, shifted(): lax.ppermute(array, axis, [(i, (i + step) % size) for i in range(size)])  49.2 us
    ppermute x19, starting transfers between devices, shifted(): lax.ppermute(array, axis, [(i, (i + step) % size) for i in range(size)])  23.7 us
    all_to_all x1, blocking collectives, block(): quarters = lax.all_to_all(partial, 'sp', 0, 0, tiled=True)  14.5 us
    unnamed x61, local copies, waits for them, and re-layouts  13.9 us
    pallas_call x2, Pallas kernels, attention(): pl.pallas_call(functools.partial(attention_kernel, slots), in_specs=in_sp...  11.5 us
    pallas_call x1, Pallas kernels, project(): pl.pallas_call(project_kernel, in_specs=[whole] * 8 + [scalars] + [whole]...  6.91 us
    pallas_call x1, Pallas kernels, output(): pl.pallas_call(output_kernel, in_specs=[pl.BlockSpec(memory_space=pltpu.S...  6.34 us
    ppermute x1, waiting for transfers between devices, block(): before = lax.ppermute(up, 'sp', along)  6.28 us
  transfers between devices with their start and end apart: 23, of which 11 were waited for; matrix products, arithmetic and copies ran while one was open for 3% of the time, Pallas kernels for 13%

profile of v1, /device:TPU:32, one launch (start us, length us, event | category | flops | bytes accessed | tf_op | source)
XLA Modules:
  0.0 152.5 jit_solution(4741125172146695799)
XLA Ops:
  0.0 4.2 %fusion = (bf16[128,1,2048]{2,1,0:T(2,128)(2,1)}, bf16[128,1,2048]{2,1,0:T(2,128)(2,1)S(1)}) fusion(bf16[128,2,2048]{2,1,0:T(2,128)(2,1)} %param.17), kind=kLoop, calls=%fused_computation.6 | loop fusion | bytes 2097152 | tf_op jit(solution)/shard_map/slice | solution.py:369
  6.4 14.5 %all_to_all.10 = f32[16,8,512]{2,1,0:T(8,128)S(1)} all-to-all(f32[16,8,512]{2,1,0:T(8,128)S(1)} %modulation.1), channel_id=1, replica_groups=mesh['sp'=16,'tp'=4,'dp'=2] {'sp'}, dimensions={0} | all-to-all | bytes 524288 | tf_op jit(solution)/shard_map/all_to_all | solution.py:378
  20.9 1.9 %collective-permute-start.6 = (f32[8,512]{1,0:T(8,128)S(1)}, f32[8,512]{1,0:T(8,128)S(1)}, u32[]{:S(2)}, u32[]{:S(2)}) collective-permute-start(f32[8,512]{1,0:T(8,128)S(1)} %reduce_sum.9.m0_ref), channel_id=1, source_target_pairs={{0,6},{2,0},{4,2},{6,4},{1,7},{3,1},{5,3},{7,5},{8,14},{10,8},{12,... | collective-permute-start | bytes 49160 | tf_op jit(solution)/shard_map/ppermute | solution.py:33
  22.8 1.8 %collective-permute-start.7 = (f32[8,512]{1,0:T(8,128)S(1)}, f32[8,512]{1,0:T(8,128)S(1)}, u32[]{:S(2)}, u32[]{:S(2)}) collective-permute-start(f32[8,512]{1,0:T(8,128)S(1)} %reduce_sum.9.m0_ref), channel_id=1, source_target_pairs={{0,4},{2,6},{4,0},{6,2},{1,5},{3,7},{5,1},{7,3},{8,12},{10,14},{12... | collective-permute-start | bytes 49160 | tf_op jit(solution)/shard_map/ppermute | solution.py:33
  31.3 9.5 %collective-permute-done.8.m3_ref = f32[8,512]{1,0:T(8,128)S(1)} collective-permute-done((f32[8,512]{1,0:T(8,128)S(1)}, f32[8,512]{1,0:T(8,128)S(1)}, u32[]{:S(2)}, u32[]{:S(2)}) %collective-permute-start.8) | collective-permute-done | bytes 16416 | tf_op jit(solution)/shard_map/ppermute | solution.py:33
  40.8 3.2 %collective-permute-start.17 = (bf16[256,2048]{1,0:T(8,128)(2,1)}, bf16[256,2048]{1,0:T(8,128)(2,1)}, u32[]{:S(2)}, u32[]{:S(2)}) collective-permute-start(bf16[256,2048]{1,0:T(8,128)(2,1)} %constant_dynamic-slice_fusion), channel_id=1, source_target_pairs={{0,6},{2,0},{4,2},{6,4},{1,7},{3,1},{5,3},{7,5},{8,14},{10,8},{12,... | collective-permute-start | bytes 3145736 | tf_op jit(solution)/shard_map/ppermute | solution.py:33
  44.9 5.8 %collective-permute-done.1.refs_3_ = bf16[128,2048]{1,0:T(8,128)(2,1)} collective-permute-done((bf16[128,2048]{1,0:T(8,128)(2,1)S(1)}, bf16[128,2048]{1,0:T(8,128)(2,1)}, u32[]{:S(2)}, u32[]{:S(2)}) %collective-permute-start.1) | collective-permute-done | bytes 524320 | tf_op jit(solution)/shard_map/ppermute | solution.py:33
  50.7 1.7 %collective-permute-start.14 = (bf16[128,2048]{1,0:T(8,128)(2,1)}, bf16[128,2048]{1,0:T(8,128)(2,1)}, u32[]{:S(2)}, u32[]{:S(2)}) collective-permute-start(bf16[128,2048]{1,0:T(8,128)(2,1)} %constant_dynamic-slice_fusion.1), channel_id=1, source_target_pairs={{0,4},{2,6},{4,0},{6,2},{1,5},{3,7},{5,1},{7,3},{8,12},{10,14},{12... | collective-permute-start | bytes 1572872 | tf_op jit(solution)/shard_map/ppermute | solution.py:33
  53.9 1.8 %collective-permute-start.5 = (bf16[128,2048]{1,0:T(8,128)(2,1)}, bf16[128,2048]{1,0:T(8,128)(2,1)}, u32[]{:S(2)}, u32[]{:S(2)}) collective-permute-start(bf16[128,2048]{1,0:T(8,128)(2,1)} %collective-permute-done.1.refs_3_), channel_id=1, source_target_pairs={{0,6},{2,0},{4,2},{6,4},{1,7},{3,1},{5,3},{7,5},{8,14},{10,8},{12,... | collective-permute-start | bytes 1572872 | tf_op jit(solution)/shard_map/ppermute | solution.py:33
  59.3 5.3 %all-to-all-start.1 = ((bf16[16,2,64,256]{3,2,1,0:T(8,128)(2,1)}), bf16[16,2,64,256]{3,2,1,0:T(8,128)(2,1)S(1)}, u32[]{:S(2)}, u32[]{:S(2)}) async-start(bf16[16,2,64,256]{3,2,1,0:T(8,128)(2,1)} %copy-done.9), calls=%async_computation.1 | async-start | bytes 2097152 | tf_op jit(solution)/shard_map/all_to_all | solution.py:387
  64.6 14.1 %collective-permute-done.14.refs_3_ = bf16[128,2048]{1,0:T(8,128)(2,1)} collective-permute-done((bf16[128,2048]{1,0:T(8,128)(2,1)}, bf16[128,2048]{1,0:T(8,128)(2,1)}, u32[]{:S(2)}, u32[]{:S(2)}) %collective-permute-start.14) | collective-permute-done | bytes 524320 | tf_op jit(solution)/shard_map/ppermute | solution.py:33
  79.6 2.5 %collective-permute-done.17.refs_6_ = bf16[256,2048]{1,0:T(8,128)(2,1)} collective-permute-done((bf16[256,2048]{1,0:T(8,128)(2,1)}, bf16[256,2048]{1,0:T(8,128)(2,1)}, u32[]{:S(2)}, u32[]{:S(2)}) %collective-permute-start.17) | collective-permute-done | bytes 1048608 | tf_op jit(solution)/shard_map/ppermute | solution.py:33
  82.1 4.0 %collective-permute-done.4.refs_6_ = bf16[128,2048]{1,0:T(8,128)(2,1)} collective-permute-done((bf16[128,2048]{1,0:T(8,128)(2,1)}, bf16[128,2048]{1,0:T(8,128)(2,1)}, u32[]{:S(2)}, u32[]{:S(2)}) %collective-permute-start.4) | collective-permute-done | bytes 524320 | tf_op jit(solution)/shard_map/ppermute | solution.py:33
  86.1 6.4 %collective-permute-done.5.refs_7_ = bf16[128,2048]{1,0:T(8,128)(2,1)} collective-permute-done((bf16[128,2048]{1,0:T(8,128)(2,1)}, bf16[128,2048]{1,0:T(8,128)(2,1)}, u32[]{:S(2)}, u32[]{:S(2)}) %collective-permute-start.5) | collective-permute-done | bytes 524320 | tf_op jit(solution)/shard_map/ppermute | solution.py:33
  98.2 6.9 %project.1 = (bf16[2,4,512,128]{3,2,1,0:T(8,128)(2,1)S(1)}, bf16[2,2,512,128]{3,2,1,0:T(8,128)(2,1)S(1)}, bf16[2,2,128,128]{3,2,1,0:T(8,128)(2,1)S(1)}, bf16[2,2,128,128]{3,2,1,0:T(8,128)(2,1)S(1)}) custom-call(bf16[128,2048]{1,0:T(8,128)(2,1)S(1)} %bitcast.16, bf16[128,2048]{1,0:T(8,128)(2,1)S(1)} %bitcast.20, ...), custom_call_target="tpu_custom_call" | custom-call | flops 3221225472 | bytes 8000000 | tf_op jit(solution)/shard_map/project/pallas_call | solution.py:137
  107.0 4.2 %collective-permute-start.10 = (bf16[2,2,128,128]{3,2,1,0:T(8,128)(2,1)S(1)}, bf16[2,2,128,128]{3,2,1,0:T(8,128)(2,1)S(1)}, u32[]{:S(2)}, u32[]{:S(2)}) collective-permute-start(bf16[2,2,128,128]{3,2,1,0:T(8,128)(2,1)S(1)} %get-tuple-element.18), channel_id=1, source_target_pairs={{8,0},{16,8},{24,16},{32,24},{40,32},{48,40},{56,48},{64,56},{72,6... | collective-permute-start | bytes 393224 | tf_op jit(solution)/shard_map/ppermute | solution.py:411
  111.1 1.9 %collective-permute-start.9 = (bf16[2,2,128,128]{3,2,1,0:T(8,128)(2,1)S(1)}, bf16[2,2,128,128]{3,2,1,0:T(8,128)(2,1)S(1)}, u32[]{:S(2)}, u32[]{:S(2)}) collective-permute-start(bf16[2,2,128,128]{3,2,1,0:T(8,128)(2,1)S(1)} %get-tuple-element.17), channel_id=1, source_target_pairs={{0,8},{8,16},{16,24},{24,32},{32,40},{40,48},{48,56},{56,64},{64,7... | collective-permute-start | bytes 393224 | tf_op jit(solution)/shard_map/ppermute | solution.py:410
  113.8 6.3 %collective-permute-done.9.before_ref = bf16[2,2,128,128]{3,2,1,0:T(8,128)(2,1)S(1)} collective-permute-done((bf16[2,2,128,128]{3,2,1,0:T(8,128)(2,1)S(1)}, bf16[2,2,128,128]{3,2,1,0:T(8,128)(2,1)S(1)}, u32[]{:S(2)}, u32[]{:S(2)}) %collective-permute-start.9) | collective-permute-done | bytes 131104 | tf_op jit(solution)/shard_map/ppermute | solution.py:410
  122.4 7.2 %shard_map.163 = (bf16[256,512]{1,0:T(8,128)(2,1)S(1)}, bf16[256,512]{1,0:T(8,128)(2,1)S(1)}, bf16[256,512]{1,0:T(8,128)(2,1)S(1)}) custom-call(s32[3]{0:T(128)S(1)} %pad_add_fusion.where_ref.refs_8_, f32[4]{0:T(128)S(1)} %copy-done.23, bf16[2,4,512,128]{3,2,1,0:T(8,128)(2,1)S(1)} %copy-done.8, bf16[2,2,512,128]{3,2,1,0:T(8,128)(2,1)S(1)} %copy-done.11, ...), custom_call_target="tpu_custom_call" | custom-call | flops 2214592512 | bytes 4000000 | tf_op jit(solution)/shard_map/pallas_call | solution.py:287
  130.5 3.4 %collective-permute-start.12 = (bf16[256,512]{1,0:T(8,128)(2,1)S(1)}, bf16[256,512]{1,0:T(8,128)(2,1)S(1)}, u32[]{:S(2)}, u32[]{:S(2)}) collective-permute-start(bf16[256,512]{1,0:T(8,128)(2,1)S(1)} %get-tuple-element.21), channel_id=1, source_target_pairs={{0,4},{2,6},{4,0},{6,2},{1,5},{3,7},{5,1},{7,3},{8,12},{10,14},{12... | collective-permute-start | bytes 786440 | tf_op jit(solution)/shard_map/ppermute | solution.py:33
  133.9 5.6 %collective-permute-done.11.refs_0_ = bf16[256,512]{1,0:T(8,128)(2,1)S(1)} collective-permute-done((bf16[256,512]{1,0:T(8,128)(2,1)S(1)}, bf16[256,512]{1,0:T(8,128)(2,1)S(1)}, u32[]{:S(2)}, u32[]{:S(2)}) %collective-permute-start.11) | collective-permute-done | bytes 262176 | tf_op jit(solution)/shard_map/ppermute | solution.py:33
  139.4 1.8 %collective-permute-start.13 = (bf16[256,512]{1,0:T(8,128)(2,1)S(1)}, bf16[256,512]{1,0:T(8,128)(2,1)S(1)}, u32[]{:S(2)}, u32[]{:S(2)}) collective-permute-start(bf16[256,512]{1,0:T(8,128)(2,1)S(1)} %get-tuple-element.22), channel_id=1, source_target_pairs={{0,6},{2,0},{4,2},{6,4},{1,7},{3,1},{5,3},{7,5},{8,14},{10,8},{12,... | collective-permute-start | bytes 786440 | tf_op jit(solution)/shard_map/ppermute | solution.py:33
  141.3 4.3 %shard_map.164.refs_11_ = bf16[256,2048]{1,0:T(8,128)(2,1)S(1)} custom-call(s32[3]{0:T(128)S(1)} %pad_add_fusion.where_ref.refs_8_, f32[4]{0:T(128)S(1)} %copy-done.23, bf16[2,4,512,128]{3,2,1,0:T(8,128)(2,1)S(1)} %copy-done.8, bf16[2,2,512,128]{3,2,1,0:T(8,128)(2,1)S(1)} %copy-done.12, bf16[2,2,128,128]{3,2,1,0:T(8,128)(2,1)S(1)} %collective-permute-done.9.before_ref, ...), custom_call_target="tpu_custom_call" | custom-call | flops 738197504 | bytes 4000000 | tf_op jit(solution)/shard_map/pallas_call | solution.py:287
  146.2 6.3 %output.1 = bf16[128,2,2048]{2,1,0:T(2,128)(2,1)} custom-call(s32[3]{0:T(128)S(1)} %pad_add_fusion.where_ref.refs_8_, bf16[256,512]{1,0:T(8,128)(2,1)S(1)} %collective-permute-done.11.refs_0_, bf16[256,512]{1,0:T(8,128)(2,1)S(1)} %collective-permute-done.12.refs_1_, bf16[256,512]{1,0:T(8,128)(2,1)S(1)} %collective-permute-done.13.refs_2_, ...), custom_call_target="tpu_custom_call" | custom-call | flops 1610612736 | bytes 10000000 | tf_op jit(solution)/shard_map/output/pallas_call | solution.py:335
  (95 shorter events, 27.7 us)
Async XLA Ops:
  4.5 36.3 %collective-permute-start.2 = (bf16[128,2048]{1,0:T(8,128)(2,1)S(1)}, bf16[128,2048]{1,0:T(8,128)(2,1)}, u32[]{:S(2)}, u32[]{:S(2)}) collective-permute-start(bf16[128,2048]{1,0:T(8,128)(2,1)S(1)} %bitcast.14), channel_id=1, source_target_pairs={{0,2},{2,4},{4,6},{6,0},{1,3},{3,5},{5,7},{7,1},{8,10},{10,12},{12... | collective-permute-start | bytes 1572872 | tf_op jit(solution)/shard_map/ppermute | solution.py:33
  20.9 7.6 %collective-permute-start.6 = (f32[8,512]{1,0:T(8,128)S(1)}, f32[8,512]{1,0:T(8,128)S(1)}, u32[]{:S(2)}, u32[]{:S(2)}) collective-permute-start(f32[8,512]{1,0:T(8,128)S(1)} %reduce_sum.9.m0_ref), channel_id=1, source_target_pairs={{0,6},{2,0},{4,2},{6,4},{1,7},{3,1},{5,3},{7,5},{8,14},{10,8},{12,... | collective-permute-start | bytes 49160 | tf_op jit(solution)/shard_map/ppermute | solution.py:33
  22.8 6.5 %collective-permute-start.7 = (f32[8,512]{1,0:T(8,128)S(1)}, f32[8,512]{1,0:T(8,128)S(1)}, u32[]{:S(2)}, u32[]{:S(2)}) collective-permute-start(f32[8,512]{1,0:T(8,128)S(1)} %reduce_sum.9.m0_ref), channel_id=1, source_target_pairs={{0,4},{2,6},{4,0},{6,2},{1,5},{3,7},{5,1},{7,3},{8,12},{10,14},{12... | collective-permute-start | bytes 49160 | tf_op jit(solution)/shard_map/ppermute | solution.py:33
  24.6 27.9 %collective-permute-start = (bf16[128,2048]{1,0:T(8,128)(2,1)S(1)}, bf16[128,2048]{1,0:T(8,128)(2,1)}, u32[]{:S(2)}, u32[]{:S(2)}) collective-permute-start(bf16[128,2048]{1,0:T(8,128)(2,1)S(1)} %bitcast.15), channel_id=1, source_target_pairs={{0,6},{2,0},{4,2},{6,4},{1,7},{3,1},{5,3},{7,5},{8,14},{10,8},{12,... | collective-permute-start | bytes 1572872 | tf_op jit(solution)/shard_map/ppermute | solution.py:33
  27.2 23.5 %collective-permute-start.1 = (bf16[128,2048]{1,0:T(8,128)(2,1)S(1)}, bf16[128,2048]{1,0:T(8,128)(2,1)}, u32[]{:S(2)}, u32[]{:S(2)}) collective-permute-start(bf16[128,2048]{1,0:T(8,128)(2,1)S(1)} %bitcast.18), channel_id=1, source_target_pairs={{0,6},{2,0},{4,2},{6,4},{1,7},{3,1},{5,3},{7,5},{8,14},{10,8},{12,... | collective-permute-start | bytes 1572872 | tf_op jit(solution)/shard_map/ppermute | solution.py:33
  28.5 25.4 %collective-permute-start.3 = (bf16[128,2048]{1,0:T(8,128)(2,1)S(1)}, bf16[128,2048]{1,0:T(8,128)(2,1)}, u32[]{:S(2)}, u32[]{:S(2)}) collective-permute-start(bf16[128,2048]{1,0:T(8,128)(2,1)S(1)} %bitcast.19), channel_id=1, source_target_pairs={{0,2},{2,4},{4,6},{6,0},{1,3},{3,5},{5,7},{7,1},{8,10},{10,12},{12... | collective-permute-start | bytes 1572872 | tf_op jit(solution)/shard_map/ppermute | solution.py:33
  29.3 11.5 %collective-permute-start.8 = (f32[8,512]{1,0:T(8,128)S(1)}, f32[8,512]{1,0:T(8,128)S(1)}, u32[]{:S(2)}, u32[]{:S(2)}) collective-permute-start(f32[8,512]{1,0:T(8,128)S(1)} %reduce_sum.9.m0_ref), channel_id=1, source_target_pairs={{0,2},{2,4},{4,6},{6,0},{1,3},{3,5},{5,7},{7,1},{8,10},{10,12},{12... | collective-permute-start | bytes 49160 | tf_op jit(solution)/shard_map/ppermute | solution.py:33
  40.8 38.8 %collective-permute-start.16 = (bf16[256,2048]{1,0:T(8,128)(2,1)}, bf16[256,2048]{1,0:T(8,128)(2,1)}, u32[]{:S(2)}, u32[]{:S(2)}) collective-permute-start(bf16[256,2048]{1,0:T(8,128)(2,1)} %constant_dynamic-slice_fusion), channel_id=1, source_target_pairs={{0,2},{2,4},{4,6},{6,0},{1,3},{3,5},{5,7},{7,1},{8,10},{10,12},{12... | collective-permute-start | bytes 3145736 | tf_op jit(solution)/shard_map/ppermute | solution.py:33
  40.8 41.2 %collective-permute-start.17 = (bf16[256,2048]{1,0:T(8,128)(2,1)}, bf16[256,2048]{1,0:T(8,128)(2,1)}, u32[]{:S(2)}, u32[]{:S(2)}) collective-permute-start(bf16[256,2048]{1,0:T(8,128)(2,1)} %constant_dynamic-slice_fusion), channel_id=1, source_target_pairs={{0,6},{2,0},{4,2},{6,4},{1,7},{3,1},{5,3},{7,5},{8,14},{10,8},{12,... | collective-permute-start | bytes 3145736 | tf_op jit(solution)/shard_map/ppermute | solution.py:33
  50.7 28.0 %collective-permute-start.14 = (bf16[128,2048]{1,0:T(8,128)(2,1)}, bf16[128,2048]{1,0:T(8,128)(2,1)}, u32[]{:S(2)}, u32[]{:S(2)}) collective-permute-start(bf16[128,2048]{1,0:T(8,128)(2,1)} %constant_dynamic-slice_fusion.1), channel_id=1, source_target_pairs={{0,4},{2,6},{4,0},{6,2},{1,5},{3,7},{5,1},{7,3},{8,12},{10,14},{12... | collective-permute-start | bytes 1572872 | tf_op jit(solution)/shard_map/ppermute | solution.py:33
  52.5 33.6 %collective-permute-start.4 = (bf16[128,2048]{1,0:T(8,128)(2,1)}, bf16[128,2048]{1,0:T(8,128)(2,1)}, u32[]{:S(2)}, u32[]{:S(2)}) collective-permute-start(bf16[128,2048]{1,0:T(8,128)(2,1)} %collective-permute-done.2.refs_4_), channel_id=1, source_target_pairs={{0,2},{2,4},{4,6},{6,0},{1,3},{3,5},{5,7},{7,1},{8,10},{10,12},{12... | collective-permute-start | bytes 1572872 | tf_op jit(solution)/shard_map/ppermute | solution.py:33
  53.9 38.6 %collective-permute-start.5 = (bf16[128,2048]{1,0:T(8,128)(2,1)}, bf16[128,2048]{1,0:T(8,128)(2,1)}, u32[]{:S(2)}, u32[]{:S(2)}) collective-permute-start(bf16[128,2048]{1,0:T(8,128)(2,1)} %collective-permute-done.1.refs_3_), channel_id=1, source_target_pairs={{0,6},{2,0},{4,2},{6,4},{1,7},{3,1},{5,3},{7,5},{8,14},{10,8},{12,... | collective-permute-start | bytes 1572872 | tf_op jit(solution)/shard_map/ppermute | solution.py:33
  57.0 35.4 %copy-start.25 = (f32[128,128]{1,0:T(8,128)S(1)}, f32[128,128]{1,0:T(8,128)}, u32[]{:S(2)}) copy-start(f32[128,128]{1,0:T(8,128)} %constant.60.clone.refs_11_) | copy-start | bytes 196612
  59.3 60.8 %all-to-all-start.1 = ((bf16[16,2,64,256]{3,2,1,0:T(8,128)(2,1)}), bf16[16,2,64,256]{3,2,1,0:T(8,128)(2,1)S(1)}, u32[]{:S(2)}, u32[]{:S(2)}) async-start(bf16[16,2,64,256]{3,2,1,0:T(8,128)(2,1)} %copy-done.9), calls=%async_computation.1 | async-start | bytes 2097152 | tf_op jit(solution)/shard_map/all_to_all | solution.py:387
  78.7 51.8 %collective-permute-start.15 = (bf16[128,2048]{1,0:T(8,128)(2,1)}, bf16[128,2048]{1,0:T(8,128)(2,1)}, u32[]{:S(2)}, u32[]{:S(2)}) collective-permute-start(bf16[128,2048]{1,0:T(8,128)(2,1)} %collective-permute-done.14.refs_3_), channel_id=1, source_target_pairs={{0,8},{1,33},{8,0},{9,41},{16,24},{17,49},{24,16},{25,57},{32,40},... | collective-permute-start | bytes 1572872 | tf_op jit(solution)/shard_map/ppermute | solution.py:397
  79.6 66.5 %collective-permute-start.20 = (bf16[256,2048]{1,0:T(8,128)(2,1)}, bf16[256,2048]{1,0:T(8,128)(2,1)}, u32[]{:S(2)}, u32[]{:S(2)}) collective-permute-start(bf16[256,2048]{1,0:T(8,128)(2,1)} %collective-permute-done.16.refs_5_), channel_id=1, source_target_pairs={{0,1},{1,0},{2,3},{3,2},{4,5},{5,4},{6,7},{7,6},{8,9},{9,8},{10,11... | collective-permute-start | bytes 3145736 | tf_op jit(solution)/shard_map/ppermute | solution.py:33
  82.1 64.1 %collective-permute-start.21 = (bf16[256,2048]{1,0:T(8,128)(2,1)}, bf16[256,2048]{1,0:T(8,128)(2,1)}, u32[]{:S(2)}, u32[]{:S(2)}) collective-permute-start(bf16[256,2048]{1,0:T(8,128)(2,1)} %collective-permute-done.17.refs_6_), channel_id=1, source_target_pairs={{0,1},{1,0},{2,3},{3,2},{4,5},{5,4},{6,7},{7,6},{8,9},{9,8},{10,11... | collective-permute-start | bytes 3145736 | tf_op jit(solution)/shard_map/ppermute | solution.py:33
  107.0 6.8 %collective-permute-start.10 = (bf16[2,2,128,128]{3,2,1,0:T(8,128)(2,1)S(1)}, bf16[2,2,128,128]{3,2,1,0:T(8,128)(2,1)S(1)}, u32[]{:S(2)}, u32[]{:S(2)}) collective-permute-start(bf16[2,2,128,128]{3,2,1,0:T(8,128)(2,1)S(1)} %get-tuple-element.18), channel_id=1, source_target_pairs={{8,0},{16,8},{24,16},{32,24},{40,32},{48,40},{56,48},{64,56},{72,6... | collective-permute-start | bytes 393224 | tf_op jit(solution)/shard_map/ppermute | solution.py:411
  111.1 9.0 %collective-permute-start.9 = (bf16[2,2,128,128]{3,2,1,0:T(8,128)(2,1)S(1)}, bf16[2,2,128,128]{3,2,1,0:T(8,128)(2,1)S(1)}, u32[]{:S(2)}, u32[]{:S(2)}) collective-permute-start(bf16[2,2,128,128]{3,2,1,0:T(8,128)(2,1)S(1)} %get-tuple-element.17), channel_id=1, source_target_pairs={{0,8},{8,16},{16,24},{24,32},{32,40},{40,48},{48,56},{56,64},{64,7... | collective-permute-start | bytes 393224 | tf_op jit(solution)/shard_map/ppermute | solution.py:410
  113.8 16.7 %collective-permute-start.18 = (bf16[128,2048]{1,0:T(8,128)(2,1)}, bf16[128,2048]{1,0:T(8,128)(2,1)}, u32[]{:S(2)}, u32[]{:S(2)}) collective-permute-start(bf16[128,2048]{1,0:T(8,128)(2,1)} %collective-permute-done.14.refs_3_), channel_id=1, source_target_pairs={{0,1},{1,0},{2,3},{3,2},{4,5},{5,4},{6,7},{7,6},{8,9},{9,8},{10,11... | collective-permute-start | bytes 1572872 | tf_op jit(solution)/shard_map/ppermute | solution.py:33
  129.6 9.8 %collective-permute-start.11 = (bf16[256,512]{1,0:T(8,128)(2,1)S(1)}, bf16[256,512]{1,0:T(8,128)(2,1)S(1)}, u32[]{:S(2)}, u32[]{:S(2)}) collective-permute-start(bf16[256,512]{1,0:T(8,128)(2,1)S(1)} %get-tuple-element.20), channel_id=1, source_target_pairs={{0,2},{2,4},{4,6},{6,0},{1,3},{3,5},{5,7},{7,1},{8,10},{10,12},{12... | collective-permute-start | bytes 786440 | tf_op jit(solution)/shard_map/ppermute | solution.py:33
  130.5 15.7 %collective-permute-start.19 = (bf16[128,2048]{1,0:T(8,128)(2,1)}, bf16[128,2048]{1,0:T(8,128)(2,1)S(1)}, u32[]{:S(2)}, u32[]{:S(2)}) collective-permute-start(bf16[128,2048]{1,0:T(8,128)(2,1)} %collective-permute-done.15.refs_4_), channel_id=1, source_target_pairs={{0,1},{1,0},{2,3},{3,2},{4,5},{5,4},{6,7},{7,6},{8,9},{9,8},{10,11... | collective-permute-start | bytes 1572872 | tf_op jit(solution)/shard_map/ppermute | solution.py:33
  130.5 15.0 %collective-permute-start.12 = (bf16[256,512]{1,0:T(8,128)(2,1)S(1)}, bf16[256,512]{1,0:T(8,128)(2,1)S(1)}, u32[]{:S(2)}, u32[]{:S(2)}) collective-permute-start(bf16[256,512]{1,0:T(8,128)(2,1)S(1)} %get-tuple-element.21), channel_id=1, source_target_pairs={{0,4},{2,6},{4,0},{6,2},{1,5},{3,7},{5,1},{7,3},{8,12},{10,14},{12... | collective-permute-start | bytes 786440 | tf_op jit(solution)/shard_map/ppermute | solution.py:33
  139.4 6.7 %collective-permute-start.13 = (bf16[256,512]{1,0:T(8,128)(2,1)S(1)}, bf16[256,512]{1,0:T(8,128)(2,1)S(1)}, u32[]{:S(2)}, u32[]{:S(2)}) collective-permute-start(bf16[256,512]{1,0:T(8,128)(2,1)S(1)} %get-tuple-element.22), channel_id=1, source_target_pairs={{0,6},{2,0},{4,2},{6,4},{1,7},{3,1},{5,3},{7,5},{8,14},{10,8},{12,... | collective-permute-start | bytes 786440 | tf_op jit(solution)/shard_map/ppermute | solution.py:33
  (28 other events, 339.3 us)

commit v2 on v1

v2 whole, which is shorter than its diff:
```python
import functools

import jax
import jax.numpy as jnp
import numpy as np
from jax import lax
from jax.experimental import pallas as pl
from jax.experimental.pallas import tpu as pltpu
from jax.sharding import PartitionSpec as P


HEAD_DIM = 128
GRID_W = 64
SEQ = 8192
EPSILON = 1e-06
NEGATIVE = -1e30
LOG2E = 1.4426950408889634

SLOT_REL = (0, 1, 3, 2)
REL_SLOT = (0, 1, 3, 2)

bf16 = jnp.bfloat16
f32 = jnp.float32
VMEM = pltpu.VMEM


def cost(flops, size, exps=0):
    return pl.CostEstimate(flops=int(flops), bytes_accessed=int(size), transcendentals=int(exps))


def in_hbm(array):
    return pltpu.with_memory_space_constraint(array, pltpu.HBM)


def shifted(array, step, axis):
    size = lax.axis_size(axis)
    return lax.ppermute(array, axis, [(i, (i + step) % size) for i in range(size)])


def modulation_kernel(cond_ref, ctx_ref, shift_ref, scale_ref, gate_ref, out_ref, both, rows):
    both[...] = jnp.zeros_like(both)
    both[0:2, :] = cond_ref[...].astype(f32)
    both[2:3, :] = ctx_ref[...].astype(f32)
    raw = both[...]
    act = (raw / (1.0 + jnp.exp(-raw))).astype(bf16)
    rows[0:3, :] = jnp.dot(act, shift_ref[...], preferred_element_type=f32)[0:3]
    rows[3:6, :] = jnp.dot(act, scale_ref[...], preferred_element_type=f32)[0:3]
    rows[6:8, :] = jnp.dot(act, gate_ref[...], preferred_element_type=f32)[0:2]
    for copy in range(out_ref.shape[0]):
        out_ref[copy] = rows[...]


def modulation(copies, condition, ctx_condition, w_shift, w_scale, w_gate):
    depth, width = w_shift.shape
    return pl.pallas_call(
        modulation_kernel,
        out_shape=jax.ShapeDtypeStruct((copies, 8, width), f32),
        scratch_shapes=[VMEM((8, depth), f32), VMEM((8, width), f32)],
        cost_estimate=cost(6e6, 3 * depth * width * 2),
        name="modulation",
        compiler_params=pltpu.CompilerParams(vmem_limit_bytes=4 << 20),
    )(condition, ctx_condition[None], w_shift, w_scale, w_gate)


def modulated_into(h_ref, row, x_ref, where, rows, gain, shift):
    step = 16
    for at in range(0, rows, step):
        x = x_ref[(*where, slice(at, at + step), slice(None))].astype(f32)
        mean = jnp.mean(x * x, axis=-1, keepdims=True)
        h = x * lax.rsqrt(mean + EPSILON) * gain + shift
        h_ref[row + at : row + at + step, :] = h.astype(bf16)


def turned(u, cosine, sine):
    lane = lax.broadcasted_iota(jnp.int32, u.shape, 1)
    swapped = jnp.where(lane % 64 < 32, pltpu.roll(u, 96, 1), pltpu.roll(u, 32, 1))
    return u * cosine + swapped * sine


def project_kernel(*refs):
    own_ref, above_ref, below_ref, across0_ref, across1_ref = refs[:5]
    where_ref, gain_ref, mod_ref, row_cos, row_sin, col_cos, col_sin = refs[5:12]
    wq_ref, wk_ref, wv_ref, q_ref, kv_ref, up_ref, down_ref = refs[12:19]
    x_all, h_ref, w_q, w_kv, q_all, kv_all, sems, out_sems = refs[19:]
    sp, tp = where_ref[0], where_ref[1]
    sources = (
        (own_ref, x_all.at[0]), (above_ref, x_all.at[1]), (below_ref, x_all.at[2]),
        (across0_ref, x_all.at[3, 0]), (across1_ref, x_all.at[3, 1]),
        (wq_ref, w_q), (wk_ref, w_kv.at[:, :HEAD_DIM]), (wv_ref, w_kv.at[:, HEAD_DIM:]),
    )
    copies = [
        pltpu.make_async_copy(source, to, sems.at[i]) for i, (source, to) in enumerate(sources)
    ]
    for copy in copies:
        copy.start()
    gains = [gain_ref[...] * (1.0 + mod_ref[3 + b : 4 + b, :]) for b in range(2)]
    left = lax.broadcasted_iota(jnp.int32, (GRID_W, HEAD_DIM), 1) < HEAD_DIM // 2

    def table(row_ref, col_ref, row):
        parts = [
            jnp.where(left, row_ref[pl.ds(row + i, 1), :], col_ref[...]) for i in range(2)
        ]
        return jnp.concatenate(parts, axis=0)

    chunks = [lax.rem(tp + SLOT_REL[c], 4) for c in range(4)]
    tables = []
    for c in range(4):
        row = sp * 8 + chunks[c] * 2
        tables.append((table(row_cos, col_cos, row), table(row_sin, col_sin, row)))
    for c in range(4):
        for copy in copies[c : c + 1] if c < 3 else copies[3:5]:
            copy.wait()
        for b in range(2):
            shift = mod_ref[b : b + 1, :]
            modulated_into(h_ref.at[c], b * 128, x_all, (c, b), 128, gains[b], shift)
    for copy in copies[5:]:
        copy.wait()
    stores = []
    for n in (2, 0, 1):
        product = jnp.dot(
            h_ref[...].reshape(1024, h_ref.shape[2]),
            w_q[:, n * 256 : n * 256 + 256] if n < 2 else w_kv[...],
            preferred_element_type=f32,
        )
        for c in range(4):
            tok = slice(c * 128, c * 128 + 128)
            for b in range(2):
                rows = slice(c * 256 + b * 128, c * 256 + b * 128 + 128)
                left_part = turned(product[rows, :128], *tables[c]).astype(bf16)
                if n < 2:
                    right_part = turned(product[rows, 128:], *tables[c]).astype(bf16)
                    q_all[2 * n, b, tok, :] = left_part
                    q_all[2 * n + 1, b, tok, :] = right_part
                else:
                    right_part = product[rows, 128:].astype(bf16)
                    kv_all[c, b, 0] = left_part
                    kv_all[c, b, 1] = right_part
        if n < 2:
            stores.append(
                pltpu.make_async_copy(
                    q_all.at[2 * n : 2 * n + 2], q_ref.at[2 * n : 2 * n + 2], out_sems.at[n]
                )
            )
            stores[-1].start()
        else:
            last = (7 - tp) % 4
            first = (4 - tp) % 4
            last = jnp.where(last >= 2, 5 - last, last)
            first = jnp.where(first >= 2, 5 - first, first)
            for i, (source, to) in enumerate(
                ((kv_all.at[last], up_ref), (kv_all.at[first], down_ref), (kv_all, kv_ref))
            ):
                stores.append(pltpu.make_async_copy(source, to, out_sems.at[2 + i]))
                stores[-1].start()
    for store in stores:
        store.wait()


def project(arrays, where, gain, mod, weights):
    width = gain.shape[1]
    whole = pl.BlockSpec(memory_space=VMEM)
    scalars = pl.BlockSpec(memory_space=pltpu.SMEM)
    far = pl.BlockSpec(memory_space=pltpu.HBM)
    shapes = [(4, 2, 512, HEAD_DIM), (4, 2, 2, 128, HEAD_DIM)] + [(2, 2, 128, HEAD_DIM)] * 2
    return pl.pallas_call(
        project_kernel,
        in_specs=[far] * 5 + [scalars] + [whole] * 6 + [far] * 3,
        out_specs=tuple(far for _ in shapes),
        out_shape=tuple(pltpu.HBM(shape, bf16) for shape in shapes),
        scratch_shapes=[
            VMEM((4, 2, 128, width), bf16),
            VMEM((4, 256, width), bf16),
            VMEM((width, 512), bf16),
            VMEM((width, 2 * HEAD_DIM), bf16),
            VMEM(shapes[0], bf16),
            VMEM(shapes[1], bf16),
            pltpu.SemaphoreType.DMA((8,)),
            pltpu.SemaphoreType.DMA((5,)),
        ],
        cost_estimate=cost(2 * 1024 * width * 768, 8e6),
        name="project",
        compiler_params=pltpu.CompilerParams(vmem_limit_bytes=28 << 20),
    )(*map(in_hbm, arrays), where, gain, mod, *rotation_tables(), *map(in_hbm, weights))


def turn_kernel(x_ref, out_ref):
    for b in range(2):
        out_ref[b] = x_ref[:, b, :]


def sample_major(array):
    rows, samples, width = array.shape
    step = rows // 4
    return pl.pallas_call(
        turn_kernel,
        grid=(4,),
        in_specs=[pl.BlockSpec((step, samples, width), lambda i: (i, 0, 0))],
        out_specs=pl.BlockSpec((samples, step, width), lambda i: (0, i, 0)),
        out_shape=pltpu.HBM((samples, rows, width), bf16),
        cost_estimate=cost(0, 4 * array.size),
        name="sample_major",
        compiler_params=pltpu.CompilerParams(vmem_limit_bytes=8 << 20),
    )(in_hbm(array))


def context_kernel(
    x_hbm, where_ref, gain_ref, m0_ref, m1_ref, m2_ref, m3_ref, wk_hbm, wv_hbm,
    out_ref, mod_ref, x_ref, w_kv, h_ref, block, in_sems, sems,
):
    rows = x_ref.shape[1]
    quarter = m0_ref.shape[1]
    loads = [
        pltpu.make_async_copy(source, to, in_sems.at[i])
        for i, (source, to) in enumerate(
            ((x_hbm, x_ref), (wk_hbm, w_kv.at[:, :HEAD_DIM]), (wv_hbm, w_kv.at[:, HEAD_DIM:]))
        )
    ]
    for load in loads:
        load.start()
    for j, m_ref in enumerate((m0_ref, m1_ref, m2_ref, m3_ref)):
        at = pl.multiple_of(lax.rem(where_ref[1] + j, 4) * quarter, quarter)
        mod_ref[:, pl.ds(at, quarter)] = m_ref[...]
    gain = gain_ref[...] * (1.0 + mod_ref[5:6, :])
    shift = mod_ref[2:3, :]
    loads[0].wait()
    for b in range(2):
        modulated_into(h_ref, b * rows, x_ref, (b,), rows, gain, shift)
    for load in loads[1:]:
        load.wait()
    part = jnp.dot(h_ref[...], w_kv[...], preferred_element_type=f32).astype(bf16)
    for b in range(2):
        block[b] = part[b * rows : (b + 1) * rows]
    copies = [
        pltpu.make_async_copy(block, out_ref.at[i], sems.at[i]) for i in range(out_ref.shape[0])
    ]
    for copy in copies:
        copy.start()
    for copy in copies:
        copy.wait()


def project_context(copies, context, where, gain, quarters, w_key, w_value):
    samples, rows, width = context.shape
    whole = pl.BlockSpec(memory_space=VMEM)
    far = pl.BlockSpec(memory_space=pltpu.HBM)
    return pl.pallas_call(
        context_kernel,
        in_specs=[far, pl.BlockSpec(memory_space=pltpu.SMEM)] + [whole] * 5 + [far] * 2,
        out_specs=(far, whole),
        out_shape=(
            pltpu.HBM((copies, samples, rows, 2 * HEAD_DIM), bf16),
            jax.ShapeDtypeStruct((8, width), f32),
        ),
        scratch_shapes=[
            VMEM((samples, rows, width), bf16),
            VMEM((width, 2 * HEAD_DIM), bf16),
            VMEM((samples * rows, width), bf16),
            VMEM((samples, rows, 2 * HEAD_DIM), bf16),
            pltpu.SemaphoreType.DMA((3,)),
            pltpu.SemaphoreType.DMA((copies,)),
        ],
        cost_estimate=cost(2 * 2 * rows * width * 256, 2 * rows * width * 2 + width * 512),
        name="project_context",
        compiler_params=pltpu.CompilerParams(vmem_limit_bytes=10 << 20),
    )(in_hbm(context), where, gain, *quarters, in_hbm(w_key), in_hbm(w_value))


def halves_kernel(below_ref, above_ref, first_ref, second_ref, buffer, sems):
    loads = [
        pltpu.make_async_copy(below_ref.at[0], buffer.at[0], sems.at[0]),
        pltpu.make_async_copy(above_ref.at[1], buffer.at[1], sems.at[1]),
    ]
    stores = [
        pltpu.make_async_copy(buffer.at[0], first_ref, sems.at[2]),
        pltpu.make_async_copy(buffer.at[1], second_ref, sems.at[3]),
    ]
    for load in loads:
        load.start()
    for load, store in zip(loads, stores):
        load.wait()
        store.start()
    for store in stores:
        store.wait()


def halves(below, above):
    far = pl.BlockSpec(memory_space=pltpu.HBM)
    shape = below.shape[1:]
    return pl.pallas_call(
        halves_kernel,
        in_specs=[far] * 2,
        out_specs=(far,) * 2,
        out_shape=(pltpu.HBM(shape, bf16),) * 2,
        scratch_shapes=[VMEM((2, *shape), bf16), pltpu.SemaphoreType.DMA((4,))],
        cost_estimate=cost(0, 4e6),
        name="halves",
        compiler_params=pltpu.CompilerParams(vmem_limit_bytes=4 << 20),
    )(in_hbm(below), in_hbm(above))


def attention_kernel(
    slots, where_ref, sink_ref, q_ref, kv_ref, before_ref, after_ref, ctx_ref, *refs
):
    if slots == (0,):
        w_ref, near, branch_ref, held = refs[0], refs[1:5], refs[5], refs[6:10]
        heads, near_sems = refs[-2:]
        moves = [
            pltpu.make_async_copy(source, to, near_sems.at[i])
            for i, (source, to) in enumerate(zip(near, held))
        ]
        for move in moves:
            move.start()
        outs, refs = (heads,), refs[10:-2]
    else:
        outs, refs = refs[: len(slots)], refs[len(slots) :]
    tile_k, tile_v, keys, values, scores, weights, q_all, kv_all, sems = refs
    copies = [pltpu.make_async_copy(kv_ref, kv_all, sems.at[0])]
    for at, slot in enumerate(slots):
        source = q_ref.at[:, :, slot * 128 : slot * 128 + 128, :]
        copies.append(pltpu.make_async_copy(source, q_all.at[at], sems.at[1 + at]))
    for copy in copies:
        copy.start()
    ctx_len = ctx_ref.shape[0] * ctx_ref.shape[2]
    span = ctx_len + 384
    sp, tp = where_ref[0], where_ref[1]
    ahead = lax.broadcasted_iota(jnp.int32, (128, 128), 1) - lax.broadcasted_iota(
        jnp.int32, (128, 128), 0
    )
    factor = HEAD_DIM ** (-0.5) * LOG2E
    across = (((1,), (1,)), ((), ()))
    values[:, :, HEAD_DIM:] = jnp.ones((2, span, HEAD_DIM), bf16)
    for b in range(2):
        keys[b, :ctx_len, :] = ctx_ref[:, b, :, :HEAD_DIM].reshape(ctx_len, HEAD_DIM)
        values[b, :ctx_len, :HEAD_DIM] = ctx_ref[:, b, :, HEAD_DIM:].reshape(ctx_len, HEAD_DIM)
    for copy in copies:
        copy.wait()
    for b in range(2):
        for tile, which in ((tile_k, 0), (tile_v, 1)):
            for c in range(4):
                tile[b, c * 128 : c * 128 + 128, :] = kv_all[c, b, which]
            tile[b, 512:640, :] = before_ref[b, which]
            tile[b, 640:768, :] = after_ref[b, which]
    units = [(at, slot, b) for at, slot in enumerate(slots) for b in range(2)]
    for at, slot, b in units:
        out_ref = outs[at]
        chunk = lax.rem(tp + SLOT_REL[slot], 4)
        prev = jnp.where(chunk == 0, 4, REL_SLOT[(SLOT_REL[slot] + 3) % 4])
        after = jnp.where(chunk == 3, 5, REL_SLOT[(SLOT_REL[slot] + 1) % 4])
        starts = (pl.multiple_of(prev * 128, 128), slot * 128, pl.multiple_of(after * 128, 128))
        for to, start in enumerate(starts):
            rows = slice(ctx_len + to * 128, ctx_len + to * 128 + 128)
            keys[b, rows, :] = tile_k[b, pl.ds(start, 128), :]
            values[b, rows, :HEAD_DIM] = tile_v[b, pl.ds(start, 128), :]
        q = q_all[at, :, b].reshape(512, HEAD_DIM)
        scores[b] = lax.dot_general(q, keys[b], across, preferred_element_type=f32)
        no_prev = (chunk == 0) & (sp == 0)
        no_after = (chunk == 3) & (sp == SEQ // 512 - 1)
        keep_prev = ahead >= jnp.where(no_prev, 1000, 0)
        keep_after = ahead <= jnp.where(no_after, -1000, 0)
        sinks = []
        for n in range(4):
            rows = slice(n * 128, n * 128 + 128)
            sink = sink_ref[n] * LOG2E

            def part(c):
                tile = scores[b, rows, c * 128 : c * 128 + 128]
                if c == ctx_len // 128:
                    tile = jnp.where(keep_prev, tile, NEGATIVE)
                if c == ctx_len // 128 + 2:
                    tile = jnp.where(keep_after, tile, NEGATIVE)
                return tile

            top = part(0)
            for c in range(1, span // 128):
                top = jnp.maximum(top, part(c))
            top = jnp.maximum(jnp.max(top, axis=-1, keepdims=True) * factor, sink)
            for c in range(span // 128):
                weights[b, rows, c * 128 : c * 128 + 128] = jnp.exp2(
                    part(c) * factor - top
                ).astype(bf16)
            sinks.append(jnp.exp2(sink - top))
        both = jnp.dot(weights[b], values[b], preferred_element_type=f32)
        for n in range(4):
            rows = slice(n * 128, n * 128 + 128)
            total = both[rows, HEAD_DIM:] + sinks[n]
            out_ref[b * 128 : b * 128 + 128, rows] = (
                both[rows, :HEAD_DIM] / total
            ).astype(bf16)
    if slots == (0,):
        part = jnp.dot(heads[...], w_ref[...], preferred_element_type=f32)
        branch_ref[...] = part.astype(bf16)
        for move in moves:
            move.wait()


def attention(slots, where, sink, q, kv, before, after, ctx, w_own=None, near=()):
    parts, _, rows, _ = ctx.shape
    ctx_len = parts * rows
    work = 2 * len(slots) * 4 * 128 * (ctx_len + 384)
    whole = pl.BlockSpec(memory_space=VMEM)
    scalars = pl.BlockSpec(memory_space=pltpu.SMEM)
    operands = [where, sink, in_hbm(q), in_hbm(kv), before, after, ctx]
    in_specs = [scalars] * 2 + [pl.BlockSpec(memory_space=pltpu.HBM)] * 2 + [whole] * 3
    span = ctx_len + 384
    scratch = [
        VMEM((2, 768, HEAD_DIM), bf16),
        VMEM((2, 768, HEAD_DIM), bf16),
        VMEM((2, span, HEAD_DIM), bf16),
        VMEM((2, span, 2 * HEAD_DIM), bf16),
        VMEM((2, 512, span), f32),
        VMEM((2, 512, span), bf16),
        VMEM((len(slots), 4, 2, 128, HEAD_DIM), bf16),
        VMEM(kv.shape, bf16),
        pltpu.SemaphoreType.DMA((1 + len(slots),)),
    ]
    shapes = [(256, 512)] * len(slots)
    if slots == (0,):
        operands += [w_own, *map(in_hbm, near)]
        in_specs += [whole] + [pl.BlockSpec(memory_space=pltpu.HBM)] * len(near)
        shapes = [(256, w_own.shape[1])] + [array.shape for array in near]
        scratch += [VMEM((256, 512), bf16), pltpu.SemaphoreType.DMA((len(near),))]
    return pl.pallas_call(
        functools.partial(attention_kernel, slots),
        in_specs=in_specs,
        out_specs=tuple(whole for _ in shapes),
        out_shape=tuple(jax.ShapeDtypeStruct(shape, bf16) for shape in shapes),
        scratch_shapes=scratch,
        cost_estimate=cost(work * 512, 4e6, work),
        compiler_params=pltpu.CompilerParams(vmem_limit_bytes=24 << 20),
    )(*operands)


def output_kernel(where_ref, *refs):
    a_refs, w_refs = refs[:3], refs[3:11]
    branch_ref, mod_ref, lat_ref, out_ref = refs[11:]
    sp, dp = where_ref[0], where_ref[2]
    odd_x, odd_z = lax.rem(sp, 2), lax.rem(lax.div(sp, 4), 2)
    at_two = []
    for core, odd in ((dp, jnp.where(dp == 0, odd_x, odd_z)), (1 - dp, jnp.where(dp == 0, odd_z, odd_x))):
        at_two += [core * 256 + odd * 128, core * 256 + (1 - odd) * 128]
    groups = (
        (a_refs[0], (2, 6), (dp * 256, 256 - dp * 256)),
        (a_refs[1], (0, 1, 4, 5), at_two),
        (a_refs[2], (3, 7), (dp * 256, 256 - dp * 256)),
    )
    heads = []
    for a_ref, pieces, starts in groups:
        parts = [
            a_ref[:, pl.ds(pl.multiple_of(start, 128), w_refs[i].shape[0])]
            for i, start in zip(pieces, starts)
        ]
        heads.append(jnp.concatenate(parts, axis=1))
    tile = 512
    for n in range(0, out_ref.shape[2], tile):
        cols = slice(n, n + tile)
        total = branch_ref[:, cols].astype(f32)
        for a, (_, pieces, _) in zip(heads, groups):
            w = jnp.concatenate([w_refs[i][:, cols] for i in pieces], axis=0)
            part = jnp.dot(a, w, preferred_element_type=f32)
            total = total + part.astype(bf16).astype(f32)
        for b in range(2):
            gate = mod_ref[6 + b : 7 + b, cols]
            mixed = lat_ref[b, :, cols].astype(f32) + gate * total[b * 128 : b * 128 + 128]
            out_ref[:, b, cols] = mixed.astype(bf16)


def output(where, attn, gathered, branch, mod, latent):
    _, rows, width = latent.shape
    whole = pl.BlockSpec(memory_space=VMEM)
    return pl.pallas_call(
        output_kernel,
        in_specs=[pl.BlockSpec(memory_space=pltpu.SMEM)] + [whole] * (len(attn) + len(gathered) + 3),
        out_specs=whole,
        out_shape=jax.ShapeDtypeStruct((rows, 2, width), bf16),
        cost_estimate=cost(2 * 256 * width * width * 3 // 4, 10e6),
        name="output",
        compiler_params=pltpu.CompilerParams(vmem_limit_bytes=12 << 20),
    )(where, *attn, *gathered, branch, mod, latent)


def rotation_tables():
    quarter = HEAD_DIM // 4
    freqs = np.float32(10000.0) ** (-np.arange(quarter, dtype=np.float32) / np.float32(quarter))
    tables = []
    for count, left in ((SEQ // GRID_W, True), (GRID_W, False)):
        angle = (np.arange(count, dtype=np.float32)[:, None] * freqs).astype(np.float64)
        cosine = np.concatenate([np.cos(angle)] * 2, axis=1)
        sine = np.concatenate([-np.sin(angle), np.sin(angle)], axis=1)
        for values in (cosine, sine):
            pair = [values, np.zeros_like(values)]
            table = np.concatenate(pair if left else pair[::-1], axis=1)
            tables.append(jnp.asarray(table.astype(np.float32)))
    return tables


def block(
    latent, context, condition, ctx_condition, norm_gain, w_shift, w_scale, w_gate,
    w_query, w_key, w_value, w_out, sink,
):
    sp, tp, dp = (lax.axis_index(name) for name in ("sp", "tp", "dp"))
    n_sp = lax.axis_size("sp")
    where = jnp.stack([sp, tp, dp]).astype(jnp.int32)

    own = jnp.moveaxis(latent, 1, 0)
    below = shifted(own, 1, "tp")
    above = shifted(own, -1, "tp")
    first, second = halves(below, above)
    across_0 = shifted(first, 1, "tp")
    across_1 = shifted(second, -1, "tp")

    partial = modulation(n_sp, condition, ctx_condition, w_shift, w_scale, w_gate)
    quarters = lax.all_to_all(partial, "sp", 0, 0, tiled=True)
    quarter = quarters.sum(axis=0)
    around = [quarter]
    for j in (1, 2, 3):
        around.append(shifted(quarter, -j, "tp"))
    gain = norm_gain[None]
    turned_context = sample_major(context)
    ctx, mod = project_context(
        n_sp, turned_context, where, gain, around, w_key, w_value
    )
    ctx = lax.all_to_all(ctx, "sp", 0, 0, tiled=True)

    half = lax.dynamic_slice_in_dim(w_out, dp * 256, 256, axis=0)
    parity = jnp.where(dp == 0, sp % 2, sp // 4 % 2)
    part = lax.dynamic_slice_in_dim(w_out, dp * 256 + parity * 128, 128, axis=0)
    pairs = []
    for s in range(n_sp):
        for d in range(2):
            pairs.append((s * 2 + d, (s ^ (1 if d == 0 else 4)) * 2 + d))
    mine = shifted(part, 2, "tp")
    theirs = lax.ppermute(mine, ("sp", "dp"), pairs)
    w_below = shifted(half, 1, "tp")
    w_above = shifted(half, -1, "tp")
    gathered = [mine, theirs, w_below, w_above]
    for array in tuple(gathered):
        gathered.append(shifted(array, 1, "dp"))

    q, kv, up, down = project(
        (own, above, below, across_0, across_1),
        where, gain, mod, (w_query, w_key, w_value),
    )

    along = [(i, i + 1) for i in range(n_sp - 1)]
    before = lax.ppermute(up, "sp", along)
    after = lax.ppermute(down, "sp", [(j, i) for i, j in along])

    attn = attention((3, 1, 2), where, sink, q, kv, before, after, ctx)
    heads = []
    for j, array in ((1, attn[1]), (2, attn[0]), (3, attn[2])):
        heads.append(shifted(array, j, "tp"))
    branch, *near = attention(
        (0,), where, sink, q, kv, before, after, ctx, w_out, gathered[:4]
    )
    return output(where, heads, near + gathered[4:], branch, mod, own)


def solution(mesh):
    return jax.shard_map(
        block,
        mesh=mesh,
        in_specs=(
            P(("sp", "tp"), "dp", None),
            P("sp", "dp", None),
            P("dp", "sp"),
            P("sp"),
            P(),
            P("sp", "tp"),
            P("sp", "tp"),
            P("sp", "tp"),
            P(None, "tp"),
            P(None, "tp"),
            P(None, "tp"),
            P("tp", None),
            P("tp"),
        ),
        out_specs=P(("sp", "tp"), "dp", None),
        check_vma=False,
    )
```

time: 153 us -> 134 us (0.88)
  the two profiles are of different devices: /device:TPU:32 before, /device:TPU:1 now
where the time goes in v2:
time: 134 us; the launch traced here: 132 us
  waiting for transfers between devices  44.4 us (33%)
  starting transfers between devices  43.9 us (33%)
  Pallas kernels  39.5 us (29%)
  local copies, waits for them, and re-layouts  3.74 us (3%)
    ppermute x17, waiting for transfers between devices, shifted(): lax.ppermute(array, axis, [(i, (i + step) % size) for i in range(size)])  30.7 us
    ppermute x17, starting transfers between devices, shifted(): lax.ppermute(array, axis, [(i, (i + step) % size) for i in range(size)])  22.2 us
    pallas_call x2, Pallas kernels, attention(): pl.pallas_call(functools.partial(attention_kernel, slots), in_specs=in_sp...  14.7 us
    pallas_call x1, Pallas kernels, project(): pl.pallas_call(project_kernel, in_specs=[far] * 5 + [scalars] + [whole] *...  9.11 us
    all_to_all x1, starting transfers between devices, block(): ctx = lax.all_to_all(ctx, 'sp', 0, 0, tiled=True)  7.61 us
    all_to_all x1, starting transfers between devices, block(): quarters = lax.all_to_all(partial, 'sp', 0, 0, tiled=True)  7.6 us
    ppermute x1, waiting for transfers between devices, block(): after = lax.ppermute(down, 'sp', [(j, i) for i, j in along])  5.67 us
    pallas_call x1, Pallas kernels, output(): pl.pallas_call(output_kernel, in_specs=[pl.BlockSpec(memory_space=pltpu.S...  5.51 us
  transfers between devices with their start and end apart: 22, of which 7 were waited for; matrix products, arithmetic and copies ran while one was open for 2% of the time, Pallas kernels for 26%

profile of v2, /device:TPU:1, one launch (start us, length us, event | category | flops | bytes accessed | tf_op | source)
XLA Modules:
  0.0 132.0 jit_solution(3757970343355947583)
XLA Ops:
  0.0 1.7 %copy.20 = bf16[128,2,2048]{2,0,1:T(8,128)(2,1)S(1)} copy(bf16[128,2,2048]{2,1,0:T(2,128)(2,1)} %param.17) | data formatting | bytes 2097152 | tf_op args[0]
  1.8 3.6 %collective-permute-start = (bf16[2,128,2048]{2,1,0:T(8,128)(2,1)S(1)}, bf16[2,128,2048]{2,1,0:T(8,128)(2,1)}, u32[]{:S(2)}, u32[]{:S(2)}) collective-permute-start(bf16[2,128,2048]{2,1,0:T(8,128)(2,1)S(1)} %bitcast.8), channel_id=1, source_target_pairs={{0,6},{2,0},{4,2},{6,4},{1,7},{3,1},{5,3},{7,5},{8,14},{10,8},{12,... | collective-permute-start | bytes 3145736 | tf_op jit(solution)/shard_map/ppermute | solution.py:37
  6.4 7.6 %all-to-all-start = ((f32[16,8,512]{2,1,0:T(8,128)}), f32[16,8,512]{2,1,0:T(8,128)S(1)}, u32[]{:S(2)}, u32[]{:S(2)}) async-start(f32[16,8,512]{2,1,0:T(8,128)} %modulation.1), calls=%async_computation | async-start | bytes 524288 | tf_op jit(solution)/shard_map/all_to_all | solution.py:512
  16.5 5.1 %all-to-all-done = f32[16,8,512]{2,1,0:T(8,128)S(1)} async-done(((f32[16,8,512]{2,1,0:T(8,128)}), f32[16,8,512]{2,1,0:T(8,128)S(1)}, u32[]{:S(2)}, u32[]{:S(2)}) %all-to-all-start) | async-done | bytes 262176 | tf_op jit(solution)/shard_map/all_to_all | solution.py:512
  21.7 2.6 %collective-permute-start.4 = (f32[8,512]{1,0:T(8,128)S(1)}, f32[8,512]{1,0:T(8,128)S(1)}, u32[]{:S(2)}, u32[]{:S(2)}) collective-permute-start(f32[8,512]{1,0:T(8,128)S(1)} %reduce_sum.9.m0_ref), channel_id=1, source_target_pairs={{0,6},{2,0},{4,2},{6,4},{1,7},{3,1},{5,3},{7,5},{8,14},{10,8},{12,... | collective-permute-start | bytes 49160 | tf_op jit(solution)/shard_map/ppermute | solution.py:37
  25.4 13.3 %collective-permute-done.4.m1_ref = f32[8,512]{1,0:T(8,128)S(1)} collective-permute-done((f32[8,512]{1,0:T(8,128)S(1)}, f32[8,512]{1,0:T(8,128)S(1)}, u32[]{:S(2)}, u32[]{:S(2)}) %collective-permute-start.4) | collective-permute-done | bytes 16416 | tf_op jit(solution)/shard_map/ppermute | solution.py:37
  38.7 3.7 %collective-permute-start.15 = (bf16[256,2048]{1,0:T(8,128)(2,1)}, bf16[256,2048]{1,0:T(8,128)(2,1)}, u32[]{:S(2)}, u32[]{:S(2)}) collective-permute-start(bf16[256,2048]{1,0:T(8,128)(2,1)} %constant_dynamic-slice_fusion), channel_id=1, source_target_pairs={{0,6},{2,0},{4,2},{6,4},{1,7},{3,1},{5,3},{7,5},{8,14},{10,8},{12,... | collective-permute-start | bytes 3145736 | tf_op jit(solution)/shard_map/ppermute | solution.py:37
  42.9 3.7 %sample_major.1.x_hbm = bf16[2,64,2048]{2,1,0:T(8,128)(2,1)} custom-call(bf16[64,2,2048]{2,1,0:T(2,128)(2,1)} %x_ref.1), custom_call_target="tpu_custom_call" | custom-call | bytes 1048576 | tf_op jit(solution)/shard_map/sample_major/pallas_call | solution.py:194
  46.7 2.1 %halves.1 = (bf16[128,2048]{1,0:T(8,128)(2,1)}, bf16[128,2048]{1,0:T(8,128)(2,1)}) custom-call(bf16[2,128,2048]{2,1,0:T(8,128)(2,1)} %collective-permute-done.1.below_ref.refs_2_, bf16[2,128,2048]{2,1,0:T(8,128)(2,1)} %collective-permute-done.above_ref.refs_1_), custom_call_target="tpu_custom_call" | custom-call | bytes 4000000 | tf_op jit(solution)/shard_map/halves/pallas_call | solution.py:289
  50.6 12.6 %collective-permute-done.5.m2_ref = f32[8,512]{1,0:T(8,128)S(1)} collective-permute-done((f32[8,512]{1,0:T(8,128)S(1)}, f32[8,512]{1,0:T(8,128)S(1)}, u32[]{:S(2)}, u32[]{:S(2)}) %collective-permute-start.5) | collective-permute-done | bytes 16416 | tf_op jit(solution)/shard_map/ppermute | solution.py:37
  63.2 2.1 %collective-permute-start.2 = (bf16[128,2048]{1,0:T(8,128)(2,1)}, bf16[128,2048]{1,0:T(8,128)(2,1)}, u32[]{:S(2)}, u32[]{:S(2)}) collective-permute-start(bf16[128,2048]{1,0:T(8,128)(2,1)} %get-tuple-element.21), channel_id=1, source_target_pairs={{0,2},{2,4},{4,6},{6,0},{1,3},{3,5},{5,7},{7,1},{8,10},{10,12},{12... | collective-permute-start | bytes 1572872 | tf_op jit(solution)/shard_map/ppermute | solution.py:37
  65.9 3.4 %project_context.1 = (bf16[16,2,64,256]{3,2,1,0:T(8,128)(2,1)}, f32[8,2048]{1,0:T(8,128)S(1)}) custom-call(bf16[2,64,2048]{2,1,0:T(8,128)(2,1)} %sample_major.1.x_hbm, s32[3]{0:T(128)S(1)} %pad_add_fusion.where_ref.refs_5_, f32[1,2048]{1,0:T(1,128)S(1)} %bitcast.12, f32[8,512]{1,0:T(8,128)S(1)} %reduce_sum.9.m0_ref, ...), custom_call_target="tpu_custom_call" | custom-call | flops 134217728 | bytes 1572864 | tf_op jit(solution)/shard_map/project_context/pallas_call | solution.py:246
  69.3 7.6 %all-to-all-start.1 = ((bf16[16,2,64,256]{3,2,1,0:T(8,128)(2,1)}), bf16[16,2,64,256]{3,2,1,0:T(8,128)(2,1)S(1)}, u32[]{:S(2)}, u32[]{:S(2)}) async-start(bf16[16,2,64,256]{3,2,1,0:T(8,128)(2,1)} %get-tuple-element.28), calls=%async_computation.1 | async-start | bytes 2097152 | tf_op jit(solution)/shard_map/all_to_all | solution.py:522
  76.9 3.3 %collective-permute-start.18 = (bf16[256,2048]{1,0:T(8,128)(2,1)}, bf16[256,2048]{1,0:T(8,128)(2,1)}, u32[]{:S(2)}, u32[]{:S(2)}) collective-permute-start(bf16[256,2048]{1,0:T(8,128)(2,1)} %collective-permute-done.14.refs_3_), channel_id=1, source_target_pairs={{0,1},{1,0},{2,3},{3,2},{4,5},{5,4},{6,7},{7,6},{8,9},{9,8},{10,11... | collective-permute-start | bytes 3145736 | tf_op jit(solution)/shard_map/ppermute | solution.py:37
  81.0 9.1 %project.1 = (bf16[4,2,512,128]{3,2,1,0:T(8,128)(2,1)}, bf16[4,2,2,128,128]{4,3,2,1,0:T(8,128)(2,1)}, bf16[2,2,128,128]{3,2,1,0:T(8,128)(2,1)}, bf16[2,2,128,128]{3,2,1,0:T(8,128)(2,1)}) custom-call(bf16[2,128,2048]{2,1,0:T(8,128)(2,1)} %bitcast.10, bf16[2,128,2048]{2,1,0:T(8,128)(2,1)} %collective-permute-done.above_ref.refs_1_, ...), custom_call_target="tpu_custom_call" | custom-call | flops 3221225472 | bytes 8000000 | tf_op jit(solution)/shard_map/project/pallas_call | solution.py:165
  90.2 3.6 %collective-permute-start.7 = (bf16[2,2,128,128]{3,2,1,0:T(8,128)(2,1)}, bf16[2,2,128,128]{3,2,1,0:T(8,128)(2,1)S(1)}, u32[]{:S(2)}, u32[]{:S(2)}) collective-permute-start(bf16[2,2,128,128]{3,2,1,0:T(8,128)(2,1)} %get-tuple-element.26), channel_id=1, source_target_pairs={{0,8},{8,16},{16,24},{24,32},{32,40},{40,48},{48,56},{56,64},{64,7... | collective-permute-start | bytes 393224 | tf_op jit(solution)/shard_map/ppermute | solution.py:545
  93.7 2.9 %collective-permute-done.7.before_ref = bf16[2,2,128,128]{3,2,1,0:T(8,128)(2,1)S(1)} collective-permute-done((bf16[2,2,128,128]{3,2,1,0:T(8,128)(2,1)}, bf16[2,2,128,128]{3,2,1,0:T(8,128)(2,1)S(1)}, u32[]{:S(2)}, u32[]{:S(2)}) %collective-permute-start.7) | collective-permute-done | bytes 131104 | tf_op jit(solution)/shard_map/ppermute | solution.py:545
  97.9 5.7 %collective-permute-done.8.after_ref = bf16[2,2,128,128]{3,2,1,0:T(8,128)(2,1)S(1)} collective-permute-done((bf16[2,2,128,128]{3,2,1,0:T(8,128)(2,1)}, bf16[2,2,128,128]{3,2,1,0:T(8,128)(2,1)S(1)}, u32[]{:S(2)}, u32[]{:S(2)}) %collective-permute-start.8) | collective-permute-done | bytes 131104 | tf_op jit(solution)/shard_map/ppermute | solution.py:546
  103.6 8.4 %shard_map.163 = (bf16[256,512]{1,0:T(8,128)(2,1)S(1)}, bf16[256,512]{1,0:T(8,128)(2,1)S(1)}, bf16[256,512]{1,0:T(8,128)(2,1)S(1)}) custom-call(s32[3]{0:T(128)S(1)} %pad_add_fusion.where_ref.refs_5_, f32[4]{0:T(128)S(1)} %copy-done.9, bf16[4,2,512,128]{3,2,1,0:T(8,128)(2,1)} %get-tuple-element.24.q_ref, ...), custom_call_target="tpu_custom_call" | custom-call | flops 2214592512 | bytes 4000000 | tf_op jit(solution)/shard_map/pallas_call | solution.py:422
  113.0 2.4 %collective-permute-start.11 = (bf16[256,512]{1,0:T(8,128)(2,1)S(1)}, bf16[256,512]{1,0:T(8,128)(2,1)S(1)}, u32[]{:S(2)}, u32[]{:S(2)}) collective-permute-start(bf16[256,512]{1,0:T(8,128)(2,1)S(1)} %get-tuple-element.31), channel_id=1, source_target_pairs={{0,6},{2,0},{4,2},{6,4},{1,7},{3,1},{5,3},{7,5},{8,14},{10,8},{12,... | collective-permute-start | bytes 786440 | tf_op jit(solution)/shard_map/ppermute | solution.py:37
  115.4 6.3 %shard_map.164 = (bf16[256,2048]{1,0:T(8,128)(2,1)S(1)}, bf16[128,2048]{1,0:T(8,128)(2,1)S(1)}, bf16[128,2048]{1,0:T(8,128)(2,1)S(1)}, bf16[256,2048]{1,0:T(8,128)(2,1)S(1)}, bf16[256,2048]{1,0:T(8,128)(2,1)S(1)}) custom-call(s32[3]{0:T(128)S(1)} %pad_add_fusion.where_ref.refs_5_, f32[4]{0:T(128)S(1)} %copy-done.9, ...), custom_call_target="tpu_custom_call" | custom-call | flops 738197504 | bytes 4000000 | tf_op jit(solution)/shard_map/pallas_call | solution.py:422
  121.7 2.4 %collective-permute-done.11.refs_2_ = bf16[256,512]{1,0:T(8,128)(2,1)S(1)} collective-permute-done((bf16[256,512]{1,0:T(8,128)(2,1)S(1)}, bf16[256,512]{1,0:T(8,128)(2,1)S(1)}, u32[]{:S(2)}, u32[]{:S(2)}) %collective-permute-start.11) | collective-permute-done | bytes 262176 | tf_op jit(solution)/shard_map/ppermute | solution.py:37
  124.1 2.4 %collective-permute-done.9.refs_0_ = bf16[256,512]{1,0:T(8,128)(2,1)S(1)} collective-permute-done((bf16[256,512]{1,0:T(8,128)(2,1)S(1)}, bf16[256,512]{1,0:T(8,128)(2,1)S(1)}, u32[]{:S(2)}, u32[]{:S(2)}) %collective-permute-start.9) | collective-permute-done | bytes 262176 | tf_op jit(solution)/shard_map/ppermute | solution.py:37
  126.5 5.5 %output.1 = bf16[128,2,2048]{2,1,0:T(2,128)(2,1)} custom-call(s32[3]{0:T(128)S(1)} %pad_add_fusion.where_ref.refs_5_, bf16[256,512]{1,0:T(8,128)(2,1)S(1)} %collective-permute-done.9.refs_0_, bf16[256,512]{1,0:T(8,128)(2,1)S(1)} %collective-permute-done.10.refs_1_, bf16[256,512]{1,0:T(8,128)(2,1)S(1)} %collective-permute-done.11.refs_2_, ...), custom_call_target="tpu_custom_call" | custom-call | flops 1610612736 | bytes 10000000 | tf_op jit(solution)/shard_map/output/pallas_call | solution.py:470
  (61 shorter events, 10.6 us)
Async XLA Ops:
  1.8 40.6 %collective-permute-start = (bf16[2,128,2048]{2,1,0:T(8,128)(2,1)S(1)}, bf16[2,128,2048]{2,1,0:T(8,128)(2,1)}, u32[]{:S(2)}, u32[]{:S(2)}) collective-permute-start(bf16[2,128,2048]{2,1,0:T(8,128)(2,1)S(1)} %bitcast.8), channel_id=1, source_target_pairs={{0,6},{2,0},{4,2},{6,4},{1,7},{3,1},{5,3},{7,5},{8,14},{10,8},{12,... | collective-permute-start | bytes 3145736 | tf_op jit(solution)/shard_map/ppermute | solution.py:37
  5.4 37.0 %collective-permute-start.1 = (bf16[2,128,2048]{2,1,0:T(8,128)(2,1)S(1)}, bf16[2,128,2048]{2,1,0:T(8,128)(2,1)}, u32[]{:S(2)}, u32[]{:S(2)}) collective-permute-start(bf16[2,128,2048]{2,1,0:T(8,128)(2,1)S(1)} %bitcast.9), channel_id=1, source_target_pairs={{0,2},{2,4},{4,6},{6,0},{1,3},{3,5},{5,7},{7,1},{8,10},{10,12},{12... | collective-permute-start | bytes 3145736 | tf_op jit(solution)/shard_map/ppermute | solution.py:37
  6.4 15.3 %all-to-all-start = ((f32[16,8,512]{2,1,0:T(8,128)}), f32[16,8,512]{2,1,0:T(8,128)S(1)}, u32[]{:S(2)}, u32[]{:S(2)}) async-start(f32[16,8,512]{2,1,0:T(8,128)} %modulation.1), calls=%async_computation | async-start | bytes 524288 | tf_op jit(solution)/shard_map/all_to_all | solution.py:512
  14.9 33.9 %collective-permute-start.12 = (bf16[128,2048]{1,0:T(8,128)(2,1)}, bf16[128,2048]{1,0:T(8,128)(2,1)}, u32[]{:S(2)}, u32[]{:S(2)}) collective-permute-start(bf16[128,2048]{1,0:T(8,128)(2,1)} %constant_dynamic-slice_fusion.1), channel_id=1, source_target_pairs={{0,4},{2,6},{4,0},{6,2},{1,5},{3,7},{5,1},{7,3},{8,12},{10,14},{12... | collective-permute-start | bytes 1572872 | tf_op jit(solution)/shard_map/ppermute | solution.py:37
  21.7 17.0 %collective-permute-start.4 = (f32[8,512]{1,0:T(8,128)S(1)}, f32[8,512]{1,0:T(8,128)S(1)}, u32[]{:S(2)}, u32[]{:S(2)}) collective-permute-start(f32[8,512]{1,0:T(8,128)S(1)} %reduce_sum.9.m0_ref), channel_id=1, source_target_pairs={{0,6},{2,0},{4,2},{6,4},{1,7},{3,1},{5,3},{7,5},{8,14},{10,8},{12,... | collective-permute-start | bytes 49160 | tf_op jit(solution)/shard_map/ppermute | solution.py:37
  25.4 40.6 %copy-start.6 = (f32[2048]{0:T(1024)S(1)}, f32[2048]{0:T(1024)}, u32[]{:S(2)}) copy-start(f32[2048]{0:T(1024)} %param.21) | copy-start | bytes 24580
  25.4 51.6 %collective-permute-start.14 = (bf16[256,2048]{1,0:T(8,128)(2,1)}, bf16[256,2048]{1,0:T(8,128)(2,1)}, u32[]{:S(2)}, u32[]{:S(2)}) collective-permute-start(bf16[256,2048]{1,0:T(8,128)(2,1)} %constant_dynamic-slice_fusion), channel_id=1, source_target_pairs={{0,2},{2,4},{4,6},{6,0},{1,3},{3,5},{5,7},{7,1},{8,10},{10,12},{12... | collective-permute-start | bytes 3145736 | tf_op jit(solution)/shard_map/ppermute | solution.py:37
  38.7 41.5 %collective-permute-start.15 = (bf16[256,2048]{1,0:T(8,128)(2,1)}, bf16[256,2048]{1,0:T(8,128)(2,1)}, u32[]{:S(2)}, u32[]{:S(2)}) collective-permute-start(bf16[256,2048]{1,0:T(8,128)(2,1)} %constant_dynamic-slice_fusion), channel_id=1, source_target_pairs={{0,6},{2,0},{4,2},{6,4},{1,7},{3,1},{5,3},{7,5},{8,14},{10,8},{12,... | collective-permute-start | bytes 3145736 | tf_op jit(solution)/shard_map/ppermute | solution.py:37
  42.4 20.8 %collective-permute-start.5 = (f32[8,512]{1,0:T(8,128)S(1)}, f32[8,512]{1,0:T(8,128)S(1)}, u32[]{:S(2)}, u32[]{:S(2)}) collective-permute-start(f32[8,512]{1,0:T(8,128)S(1)} %reduce_sum.9.m0_ref), channel_id=1, source_target_pairs={{0,4},{2,6},{4,0},{6,2},{1,5},{3,7},{5,1},{7,3},{8,12},{10,14},{12... | collective-permute-start | bytes 49160 | tf_op jit(solution)/shard_map/ppermute | solution.py:37
  42.4 22.9 %collective-permute-start.6 = (f32[8,512]{1,0:T(8,128)S(1)}, f32[8,512]{1,0:T(8,128)S(1)}, u32[]{:S(2)}, u32[]{:S(2)}) collective-permute-start(f32[8,512]{1,0:T(8,128)S(1)} %reduce_sum.9.m0_ref), channel_id=1, source_target_pairs={{0,2},{2,4},{4,6},{6,0},{1,3},{3,5},{5,7},{7,1},{8,10},{10,12},{12... | collective-permute-start | bytes 49160 | tf_op jit(solution)/shard_map/ppermute | solution.py:37
  48.8 32.2 %copy-start.10 = (f32[128,128]{1,0:T(8,128)S(1)}, f32[128,128]{1,0:T(8,128)}, u32[]{:S(2)}) copy-start(f32[128,128]{1,0:T(8,128)} %constant.60.clone.refs_8_) | copy-start | bytes 196612
  48.9 31.5 %collective-permute-start.13 = (bf16[128,2048]{1,0:T(8,128)(2,1)}, bf16[128,2048]{1,0:T(8,128)(2,1)}, u32[]{:S(2)}, u32[]{:S(2)}) collective-permute-start(bf16[128,2048]{1,0:T(8,128)(2,1)} %collective-permute-done.12.refs_1_), channel_id=1, source_target_pairs={{0,8},{1,33},{8,0},{9,41},{16,24},{17,49},{24,16},{25,57},{32,40},... | collective-permute-start | bytes 1572872 | tf_op jit(solution)/shard_map/ppermute | solution.py:532
  63.2 17.6 %collective-permute-start.2 = (bf16[128,2048]{1,0:T(8,128)(2,1)}, bf16[128,2048]{1,0:T(8,128)(2,1)}, u32[]{:S(2)}, u32[]{:S(2)}) collective-permute-start(bf16[128,2048]{1,0:T(8,128)(2,1)} %get-tuple-element.21), channel_id=1, source_target_pairs={{0,2},{2,4},{4,6},{6,0},{1,3},{3,5},{5,7},{7,1},{8,10},{10,12},{12... | collective-permute-start | bytes 1572872 | tf_op jit(solution)/shard_map/ppermute | solution.py:37
  65.3 15.7 %collective-permute-start.3 = (bf16[128,2048]{1,0:T(8,128)(2,1)}, bf16[128,2048]{1,0:T(8,128)(2,1)}, u32[]{:S(2)}, u32[]{:S(2)}) collective-permute-start(bf16[128,2048]{1,0:T(8,128)(2,1)} %get-tuple-element.22), channel_id=1, source_target_pairs={{0,6},{2,0},{4,2},{6,4},{1,7},{3,1},{5,3},{7,5},{8,14},{10,8},{12,... | collective-permute-start | bytes 1572872 | tf_op jit(solution)/shard_map/ppermute | solution.py:37
  69.3 28.6 %all-to-all-start.1 = ((bf16[16,2,64,256]{3,2,1,0:T(8,128)(2,1)}), bf16[16,2,64,256]{3,2,1,0:T(8,128)(2,1)S(1)}, u32[]{:S(2)}, u32[]{:S(2)}) async-start(bf16[16,2,64,256]{3,2,1,0:T(8,128)(2,1)} %get-tuple-element.28), calls=%async_computation.1 | async-start | bytes 2097152 | tf_op jit(solution)/shard_map/all_to_all | solution.py:522
  76.9 49.6 %collective-permute-start.18 = (bf16[256,2048]{1,0:T(8,128)(2,1)}, bf16[256,2048]{1,0:T(8,128)(2,1)}, u32[]{:S(2)}, u32[]{:S(2)}) collective-permute-start(bf16[256,2048]{1,0:T(8,128)(2,1)} %collective-permute-done.14.refs_3_), channel_id=1, source_target_pairs={{0,1},{1,0},{2,3},{3,2},{4,5},{5,4},{6,7},{7,6},{8,9},{9,8},{10,11... | collective-permute-start | bytes 3145736 | tf_op jit(solution)/shard_map/ppermute | solution.py:37
  80.2 46.3 %collective-permute-start.19 = (bf16[256,2048]{1,0:T(8,128)(2,1)}, bf16[256,2048]{1,0:T(8,128)(2,1)}, u32[]{:S(2)}, u32[]{:S(2)}) collective-permute-start(bf16[256,2048]{1,0:T(8,128)(2,1)} %collective-permute-done.15.refs_4_), channel_id=1, source_target_pairs={{0,1},{1,0},{2,3},{3,2},{4,5},{5,4},{6,7},{7,6},{8,9},{9,8},{10,11... | collective-permute-start | bytes 3145736 | tf_op jit(solution)/shard_map/ppermute | solution.py:37
  80.3 32.7 %collective-permute-start.16 = (bf16[128,2048]{1,0:T(8,128)(2,1)}, bf16[128,2048]{1,0:T(8,128)(2,1)}, u32[]{:S(2)}, u32[]{:S(2)}) collective-permute-start(bf16[128,2048]{1,0:T(8,128)(2,1)} %collective-permute-done.12.refs_1_), channel_id=1, source_target_pairs={{0,1},{1,0},{2,3},{3,2},{4,5},{5,4},{6,7},{7,6},{8,9},{9,8},{10,11... | collective-permute-start | bytes 1572872 | tf_op jit(solution)/shard_map/ppermute | solution.py:37
  80.7 34.6 %collective-permute-start.17 = (bf16[128,2048]{1,0:T(8,128)(2,1)}, bf16[128,2048]{1,0:T(8,128)(2,1)}, u32[]{:S(2)}, u32[]{:S(2)}) collective-permute-start(bf16[128,2048]{1,0:T(8,128)(2,1)} %collective-permute-done.13.refs_2_), channel_id=1, source_target_pairs={{0,1},{1,0},{2,3},{3,2},{4,5},{5,4},{6,7},{7,6},{8,9},{9,8},{10,11... | collective-permute-start | bytes 1572872 | tf_op jit(solution)/shard_map/ppermute | solution.py:37
  90.2 6.5 %collective-permute-start.7 = (bf16[2,2,128,128]{3,2,1,0:T(8,128)(2,1)}, bf16[2,2,128,128]{3,2,1,0:T(8,128)(2,1)S(1)}, u32[]{:S(2)}, u32[]{:S(2)}) collective-permute-start(bf16[2,2,128,128]{3,2,1,0:T(8,128)(2,1)} %get-tuple-element.26), channel_id=1, source_target_pairs={{0,8},{8,16},{16,24},{24,32},{32,40},{40,48},{48,56},{56,64},{64,7... | collective-permute-start | bytes 393224 | tf_op jit(solution)/shard_map/ppermute | solution.py:545
  96.6 7.0 %collective-permute-start.8 = (bf16[2,2,128,128]{3,2,1,0:T(8,128)(2,1)}, bf16[2,2,128,128]{3,2,1,0:T(8,128)(2,1)S(1)}, u32[]{:S(2)}, u32[]{:S(2)}) collective-permute-start(bf16[2,2,128,128]{3,2,1,0:T(8,128)(2,1)} %get-tuple-element.27), channel_id=1, source_target_pairs={{8,0},{16,8},{24,16},{32,24},{40,32},{48,40},{56,48},{64,56},{72,6... | collective-permute-start | bytes 393224 | tf_op jit(solution)/shard_map/ppermute | solution.py:546
  112.0 9.6 %collective-permute-start.10 = (bf16[256,512]{1,0:T(8,128)(2,1)S(1)}, bf16[256,512]{1,0:T(8,128)(2,1)S(1)}, u32[]{:S(2)}, u32[]{:S(2)}) collective-permute-start(bf16[256,512]{1,0:T(8,128)(2,1)S(1)} %get-tuple-element.30), channel_id=1, source_target_pairs={{0,4},{2,6},{4,0},{6,2},{1,5},{3,7},{5,1},{7,3},{8,12},{10,14},{12... | collective-permute-start | bytes 786440 | tf_op jit(solution)/shard_map/ppermute | solution.py:37
  113.0 11.1 %collective-permute-start.11 = (bf16[256,512]{1,0:T(8,128)(2,1)S(1)}, bf16[256,512]{1,0:T(8,128)(2,1)S(1)}, u32[]{:S(2)}, u32[]{:S(2)}) collective-permute-start(bf16[256,512]{1,0:T(8,128)(2,1)S(1)} %get-tuple-element.31), channel_id=1, source_target_pairs={{0,6},{2,0},{4,2},{6,4},{1,7},{3,1},{5,3},{7,5},{8,14},{10,8},{12,... | collective-permute-start | bytes 786440 | tf_op jit(solution)/shard_map/ppermute | solution.py:37
  115.4 11.1 %collective-permute-start.9 = (bf16[256,512]{1,0:T(8,128)(2,1)S(1)}, bf16[256,512]{1,0:T(8,128)(2,1)S(1)}, u32[]{:S(2)}, u32[]{:S(2)}) collective-permute-start(bf16[256,512]{1,0:T(8,128)(2,1)S(1)} %get-tuple-element.29), channel_id=1, source_target_pairs={{0,2},{2,4},{4,6},{6,0},{1,3},{3,5},{5,7},{7,1},{8,10},{10,12},{12... | collective-permute-start | bytes 786440 | tf_op jit(solution)/shard_map/ppermute | solution.py:37
  (12 other events, 194.9 us)

commit v3 on v2

--- a/solution.py
+++ b/solution.py
@@ -78,14 +78,13 @@
 
 
 def project_kernel(*refs):
-    own_ref, above_ref, below_ref, across0_ref, across1_ref = refs[:5]
-    where_ref, gain_ref, mod_ref, row_cos, row_sin, col_cos, col_sin = refs[5:12]
-    wq_ref, wk_ref, wv_ref, q_ref, kv_ref, up_ref, down_ref = refs[12:19]
-    x_all, h_ref, w_q, w_kv, q_all, kv_all, sems, out_sems = refs[19:]
+    x_refs = refs[:8]
+    where_ref, gain_ref, mod_ref, row_cos, row_sin, col_cos, col_sin = refs[8:15]
+    wq_ref, wk_ref, wv_ref, q_ref, kv_ref, up_ref, down_ref = refs[15:22]
+    x_all, h_ref, w_q, w_kv, q_all, kv_all, sems, out_sems = refs[22:]
     sp, tp = where_ref[0], where_ref[1]
     sources = (
-        (own_ref, x_all.at[0]), (above_ref, x_all.at[1]), (below_ref, x_all.at[2]),
-        (across0_ref, x_all.at[3, 0]), (across1_ref, x_all.at[3, 1]),
+        *((x_ref, x_all.at[i // 2, i % 2]) for i, x_ref in enumerate(x_refs)),
         (wq_ref, w_q), (wk_ref, w_kv.at[:, :HEAD_DIM]), (wv_ref, w_kv.at[:, HEAD_DIM:]),
     )
     copies = [
@@ -108,12 +107,11 @@
         row = sp * 8 + chunks[c] * 2
         tables.append((table(row_cos, col_cos, row), table(row_sin, col_sin, row)))
     for c in range(4):
-        for copy in copies[c : c + 1] if c < 3 else copies[3:5]:
-            copy.wait()
         for b in range(2):
+            copies[2 * c + b].wait()
             shift = mod_ref[b : b + 1, :]
             modulated_into(h_ref.at[c], b * 128, x_all, (c, b), 128, gains[b], shift)
-    for copy in copies[5:]:
+    for copy in copies[8:]:
         copy.wait()
     stores = []
     for n in (2, 0, 1):
@@ -164,7 +162,7 @@
     shapes = [(4, 2, 512, HEAD_DIM), (4, 2, 2, 128, HEAD_DIM)] + [(2, 2, 128, HEAD_DIM)] * 2
     return pl.pallas_call(
         project_kernel,
-        in_specs=[far] * 5 + [scalars] + [whole] * 6 + [far] * 3,
+        in_specs=[far] * 8 + [scalars] + [whole] * 6 + [far] * 3,
         out_specs=tuple(far for _ in shapes),
         out_shape=tuple(pltpu.HBM(shape, bf16) for shape in shapes),
         scratch_shapes=[
@@ -174,33 +172,13 @@
             VMEM((width, 2 * HEAD_DIM), bf16),
             VMEM(shapes[0], bf16),
             VMEM(shapes[1], bf16),
-            pltpu.SemaphoreType.DMA((8,)),
+            pltpu.SemaphoreType.DMA((11,)),
             pltpu.SemaphoreType.DMA((5,)),
         ],
         cost_estimate=cost(2 * 1024 * width * 768, 8e6),
         name="project",
         compiler_params=pltpu.CompilerParams(vmem_limit_bytes=28 << 20),
     )(*map(in_hbm, arrays), where, gain, mod, *rotation_tables(), *map(in_hbm, weights))
-
-
-def turn_kernel(x_ref, out_ref):
-    for b in range(2):
-        out_ref[b] = x_ref[:, b, :]
-
-
-def sample_major(array):
-    rows, samples, width = array.shape
-    step = rows // 4
-    return pl.pallas_call(
-        turn_kernel,
-        grid=(4,),
-        in_specs=[pl.BlockSpec((step, samples, width), lambda i: (i, 0, 0))],
-        out_specs=pl.BlockSpec((samples, step, width), lambda i: (0, i, 0)),
-        out_shape=pltpu.HBM((samples, rows, width), bf16),
-        cost_estimate=cost(0, 4 * array.size),
-        name="sample_major",
-        compiler_params=pltpu.CompilerParams(vmem_limit_bytes=8 << 20),
-    )(in_hbm(array))
 
 
 def context_kernel(
@@ -265,10 +243,9 @@
     )(in_hbm(context), where, gain, *quarters, in_hbm(w_key), in_hbm(w_value))
 
 
-def halves_kernel(below_ref, above_ref, first_ref, second_ref, buffer, sems):
+def halves_kernel(own_ref, first_ref, second_ref, buffer, sems):
     loads = [
-        pltpu.make_async_copy(below_ref.at[0], buffer.at[0], sems.at[0]),
-        pltpu.make_async_copy(above_ref.at[1], buffer.at[1], sems.at[1]),
+        pltpu.make_async_copy(own_ref.at[b], buffer.at[b], sems.at[b]) for b in range(2)
     ]
     stores = [
         pltpu.make_async_copy(buffer.at[0], first_ref, sems.at[2]),
@@ -283,19 +260,19 @@
         store.wait()
 
 
-def halves(below, above):
+def halves(own):
     far = pl.BlockSpec(memory_space=pltpu.HBM)
-    shape = below.shape[1:]
+    shape = own.shape[1:]
     return pl.pallas_call(
         halves_kernel,
-        in_specs=[far] * 2,
+        in_specs=[far],
         out_specs=(far,) * 2,
         out_shape=(pltpu.HBM(shape, bf16),) * 2,
         scratch_shapes=[VMEM((2, *shape), bf16), pltpu.SemaphoreType.DMA((4,))],
         cost_estimate=cost(0, 4e6),
         name="halves",
         compiler_params=pltpu.CompilerParams(vmem_limit_bytes=4 << 20),
-    )(in_hbm(below), in_hbm(above))
+    )(in_hbm(own))
 
 
 def attention_kernel(
@@ -502,11 +479,13 @@
     where = jnp.stack([sp, tp, dp]).astype(jnp.int32)
 
     own = jnp.moveaxis(latent, 1, 0)
-    below = shifted(own, 1, "tp")
-    above = shifted(own, -1, "tp")
-    first, second = halves(below, above)
-    across_0 = shifted(first, 1, "tp")
-    across_1 = shifted(second, -1, "tp")
+    own_0, own_1 = halves(own)
+    below_0 = shifted(own_0, 1, "tp")
+    above_1 = shifted(own_1, -1, "tp")
+    below_1 = shifted(own_1, 1, "tp")
+    above_0 = shifted(own_0, -1, "tp")
+    across_0 = shifted(below_0, 1, "tp")
+    across_1 = shifted(above_1, -1, "tp")
 
     partial = modulation(n_sp, condition, ctx_condition, w_shift, w_scale, w_gate)
     quarters = lax.all_to_all(partial, "sp", 0, 0, tiled=True)
@@ -515,7 +494,7 @@
     for j in (1, 2, 3):
         around.append(shifted(quarter, -j, "tp"))
     gain = norm_gain[None]
-    turned_context = sample_major(context)
+    turned_context = jnp.moveaxis(context, 1, 0)
     ctx, mod = project_context(
         n_sp, turned_context, where, gain, around, w_key, w_value
     )
@@ -537,7 +516,7 @@
         gathered.append(shifted(array, 1, "dp"))
 
     q, kv, up, down = project(
-        (own, above, below, across_0, across_1),
+        (own_0, own_1, above_0, above_1, below_0, below_1, across_0, across_1),
         where, gain, mod, (w_query, w_key, w_value),
     )
 

time: 134 us -> 145 us (1.082)
  the two profiles are of different devices: /device:TPU:1 before, /device:TPU:10 now
where the time goes in v3:
time: 145 us; the launch traced here: 144 us
  waiting for transfers between devices  42.2 us (29%)
  starting transfers between devices  42 us (29%)
  Pallas kernels  34.8 us (24%)
  blocking collectives  15.6 us (11%)
  local copies, waits for them, and re-layouts  9.38 us (6%)
    ppermute x19, waiting for transfers between devices, shifted(): lax.ppermute(array, axis, [(i, (i + step) % size) for i in range(size)])  37.9 us
    ppermute x19, starting transfers between devices, shifted(): lax.ppermute(array, axis, [(i, (i + step) % size) for i in range(size)])  30 us
    all_to_all x1, blocking collectives, block(): quarters = lax.all_to_all(partial, 'sp', 0, 0, tiled=True)  15.6 us
    pallas_call x2, Pallas kernels, attention(): pl.pallas_call(functools.partial(attention_kernel, slots), in_specs=in_sp...  14.7 us
    pallas_call x1, Pallas kernels, project(): pl.pallas_call(project_kernel, in_specs=[far] * 8 + [scalars] + [whole] *...  9.04 us
    unnamed x32, local copies, waits for them, and re-layouts  6.34 us
    pallas_call x1, Pallas kernels, output(): pl.pallas_call(output_kernel, in_specs=[pl.BlockSpec(memory_space=pltpu.S...  5.31 us
    all_to_all x1, starting transfers between devices, block(): ctx = lax.all_to_all(ctx, 'sp', 0, 0, tiled=True)  4.92 us
  transfers between devices with their start and end apart: 23, of which 7 were waited for; matrix products, arithmetic and copies ran while one was open for 2% of the time, Pallas kernels for 20%

profile of v3, /device:TPU:10, one launch (start us, length us, event | category | flops | bytes accessed | tf_op | source)
XLA Modules:
  0.0 144.2 jit_solution(16818211015831668865)
XLA Ops:
  0.0 2.0 %constant_dynamic-slice_fusion.1 = bf16[128,2048]{1,0:T(8,128)(2,1)} fusion(bf16[512,2048]{1,0:T(8,128)(2,1)} %refs_0_.1, s32[]{:T(128)S(6)} %select_n.28), kind=kLoop, calls=%fused_computation.4 | loop fusion | bytes 1048580 | tf_op jit(solution)/shard_map/dynamic_slice | solution.py:505
  2.0 2.3 %collective-permute-start.14 = (bf16[128,2048]{1,0:T(8,128)(2,1)}, bf16[128,2048]{1,0:T(8,128)(2,1)}, u32[]{:S(2)}, u32[]{:S(2)}) collective-permute-start(bf16[128,2048]{1,0:T(8,128)(2,1)} %constant_dynamic-slice_fusion.1), channel_id=1, source_target_pairs={{0,4},{2,6},{4,0},{6,2},{1,5},{3,7},{5,1},{7,3},{8,12},{10,14},{12... | collective-permute-start | bytes 1572872 | tf_op jit(solution)/shard_map/ppermute | solution.py:37
  8.5 15.6 %all_to_all.10 = f32[16,8,512]{2,1,0:T(8,128)S(1)} all-to-all(f32[16,8,512]{2,1,0:T(8,128)S(1)} %modulation.1), channel_id=1, replica_groups=mesh['sp'=16,'tp'=4,'dp'=2] {'sp'}, dimensions={0} | all-to-all | bytes 524288 | tf_op jit(solution)/shard_map/all_to_all | solution.py:491
  26.9 2.1 %halves.1 = (bf16[128,2048]{1,0:T(8,128)(2,1)}, bf16[128,2048]{1,0:T(8,128)(2,1)}) custom-call(bf16[2,128,2048]{2,1,0:T(8,128)(2,1)} %bitcast.11), custom_call_target="tpu_custom_call" | custom-call | bytes 4000000 | tf_op jit(solution)/shard_map/halves/pallas_call | solution.py:266
  29.0 2.6 %collective-permute-start.2 = (bf16[128,2048]{1,0:T(8,128)(2,1)}, bf16[128,2048]{1,0:T(8,128)(2,1)}, u32[]{:S(2)}, u32[]{:S(2)}) collective-permute-start(bf16[128,2048]{1,0:T(8,128)(2,1)} %get-tuple-element.21.refs_0_), channel_id=1, source_target_pairs={{0,2},{2,4},{4,6},{6,0},{1,3},{3,5},{5,7},{7,1},{8,10},{10,12},{12... | collective-permute-start | bytes 1572872 | tf_op jit(solution)/shard_map/ppermute | solution.py:37
  31.9 3.2 %collective-permute-start.1 = (bf16[128,2048]{1,0:T(8,128)(2,1)}, bf16[128,2048]{1,0:T(8,128)(2,1)}, u32[]{:S(2)}, u32[]{:S(2)}) collective-permute-start(bf16[128,2048]{1,0:T(8,128)(2,1)} %get-tuple-element.22.refs_1_), channel_id=1, source_target_pairs={{0,6},{2,0},{4,2},{6,4},{1,7},{3,1},{5,3},{7,5},{8,14},{10,8},{12,... | collective-permute-start | bytes 1572872 | tf_op jit(solution)/shard_map/ppermute | solution.py:37
  36.2 6.2 %collective-permute-done.8.m3_ref = f32[8,512]{1,0:T(8,128)S(1)} collective-permute-done((f32[8,512]{1,0:T(8,128)S(1)}, f32[8,512]{1,0:T(8,128)S(1)}, u32[]{:S(2)}, u32[]{:S(2)}) %collective-permute-start.8) | collective-permute-done | bytes 16416 | tf_op jit(solution)/shard_map/ppermute | solution.py:37
  42.3 1.6 %collective-permute-start.16 = (bf16[256,2048]{1,0:T(8,128)(2,1)}, bf16[256,2048]{1,0:T(8,128)(2,1)}, u32[]{:S(2)}, u32[]{:S(2)}) collective-permute-start(bf16[256,2048]{1,0:T(8,128)(2,1)} %constant_dynamic-slice_fusion), channel_id=1, source_target_pairs={{0,2},{2,4},{4,6},{6,0},{1,3},{3,5},{5,7},{7,1},{8,10},{10,12},{12... | collective-permute-start | bytes 3145736 | tf_op jit(solution)/shard_map/ppermute | solution.py:37
  46.0 12.0 %collective-permute-done.1.refs_3_ = bf16[128,2048]{1,0:T(8,128)(2,1)} collective-permute-done((bf16[128,2048]{1,0:T(8,128)(2,1)}, bf16[128,2048]{1,0:T(8,128)(2,1)}, u32[]{:S(2)}, u32[]{:S(2)}) %collective-permute-start.1) | collective-permute-done | bytes 524320 | tf_op jit(solution)/shard_map/ppermute | solution.py:37
  61.0 3.4 %project_context.1 = (bf16[16,2,64,256]{3,2,1,0:T(8,128)(2,1)}, f32[8,2048]{1,0:T(8,128)S(1)}) custom-call(bf16[2,64,2048]{2,1,0:T(8,128)(2,1)} %bitcast.16, s32[3]{0:T(128)S(1)} %pad_add_fusion.where_ref.refs_8_, f32[1,2048]{1,0:T(1,128)S(1)} %bitcast.13, f32[8,512]{1,0:T(8,128)S(1)} %reduce_sum.9.m0_ref, f32[8,512]{1,0:T(8,128)S(1)} %collective-permute-done.6.m1_ref, ...), custom_call_target="tpu_custom_call" | custom-call | flops 134217728 | bytes 1572864 | tf_op jit(solution)/shard_map/project_context/pallas_call | solution.py:224
  64.4 4.9 %all-to-all-start.1 = ((bf16[16,2,64,256]{3,2,1,0:T(8,128)(2,1)}), bf16[16,2,64,256]{3,2,1,0:T(8,128)(2,1)S(1)}, u32[]{:S(2)}, u32[]{:S(2)}) async-start(bf16[16,2,64,256]{3,2,1,0:T(8,128)(2,1)} %get-tuple-element.28), calls=%async_computation.1 | async-start | bytes 2097152 | tf_op jit(solution)/shard_map/all_to_all | solution.py:501
  69.3 11.5 %collective-permute-done.3.refs_5_ = bf16[128,2048]{1,0:T(8,128)(2,1)} collective-permute-done((bf16[128,2048]{1,0:T(8,128)(2,1)}, bf16[128,2048]{1,0:T(8,128)(2,1)}, u32[]{:S(2)}, u32[]{:S(2)}) %collective-permute-start.3) | collective-permute-done | bytes 524320 | tf_op jit(solution)/shard_map/ppermute | solution.py:37
  82.7 5.8 %collective-permute-done.4.refs_6_ = bf16[128,2048]{1,0:T(8,128)(2,1)} collective-permute-done((bf16[128,2048]{1,0:T(8,128)(2,1)}, bf16[128,2048]{1,0:T(8,128)(2,1)}, u32[]{:S(2)}, u32[]{:S(2)}) %collective-permute-start.4) | collective-permute-done | bytes 524320 | tf_op jit(solution)/shard_map/ppermute | solution.py:37
  88.5 9.0 %project.1 = (bf16[4,2,512,128]{3,2,1,0:T(8,128)(2,1)}, bf16[4,2,2,128,128]{4,3,2,1,0:T(8,128)(2,1)}, bf16[2,2,128,128]{3,2,1,0:T(8,128)(2,1)}, bf16[2,2,128,128]{3,2,1,0:T(8,128)(2,1)}) custom-call(bf16[128,2048]{1,0:T(8,128)(2,1)} %get-tuple-element.21.refs_0_, bf16[128,2048]{1,0:T(8,128)(2,1)} %get-tuple-element.22.refs_1_, ...), custom_call_target="tpu_custom_call" | custom-call | flops 3221225472 | bytes 8000000 | tf_op jit(solution)/shard_map/project/pallas_call | solution.py:163
  97.6 3.0 %collective-permute-start.10 = (bf16[2,2,128,128]{3,2,1,0:T(8,128)(2,1)}, bf16[2,2,128,128]{3,2,1,0:T(8,128)(2,1)S(1)}, u32[]{:S(2)}, u32[]{:S(2)}) collective-permute-start(bf16[2,2,128,128]{3,2,1,0:T(8,128)(2,1)} %get-tuple-element.27), channel_id=1, source_target_pairs={{8,0},{16,8},{24,16},{32,24},{40,32},{48,40},{56,48},{64,56},{72,6... | collective-permute-start | bytes 393224 | tf_op jit(solution)/shard_map/ppermute | solution.py:525
  100.6 2.8 %collective-permute-start.9 = (bf16[2,2,128,128]{3,2,1,0:T(8,128)(2,1)}, bf16[2,2,128,128]{3,2,1,0:T(8,128)(2,1)S(1)}, u32[]{:S(2)}, u32[]{:S(2)}) collective-permute-start(bf16[2,2,128,128]{3,2,1,0:T(8,128)(2,1)} %get-tuple-element.26), channel_id=1, source_target_pairs={{0,8},{8,16},{16,24},{24,32},{32,40},{40,48},{48,56},{56,64},{64,7... | collective-permute-start | bytes 393224 | tf_op jit(solution)/shard_map/ppermute | solution.py:524
  104.7 3.0 %collective-permute-done.9.before_ref = bf16[2,2,128,128]{3,2,1,0:T(8,128)(2,1)S(1)} collective-permute-done((bf16[2,2,128,128]{3,2,1,0:T(8,128)(2,1)}, bf16[2,2,128,128]{3,2,1,0:T(8,128)(2,1)S(1)}, u32[]{:S(2)}, u32[]{:S(2)}) %collective-permute-start.9) | collective-permute-done | bytes 131104 | tf_op jit(solution)/shard_map/ppermute | solution.py:524
  107.7 8.4 %shard_map.163 = (bf16[256,512]{1,0:T(8,128)(2,1)S(1)}, bf16[256,512]{1,0:T(8,128)(2,1)S(1)}, bf16[256,512]{1,0:T(8,128)(2,1)S(1)}) custom-call(s32[3]{0:T(128)S(1)} %pad_add_fusion.where_ref.refs_8_, f32[4]{0:T(128)S(1)} %copy-done.8, bf16[4,2,512,128]{3,2,1,0:T(8,128)(2,1)} %get-tuple-element.24.q_ref, ...), custom_call_target="tpu_custom_call" | custom-call | flops 2214592512 | bytes 4000000 | tf_op jit(solution)/shard_map/pallas_call | solution.py:399
  116.2 1.8 %collective-permute-start.11 = (bf16[256,512]{1,0:T(8,128)(2,1)S(1)}, bf16[256,512]{1,0:T(8,128)(2,1)S(1)}, u32[]{:S(2)}, u32[]{:S(2)}) collective-permute-start(bf16[256,512]{1,0:T(8,128)(2,1)S(1)} %get-tuple-element.29), channel_id=1, source_target_pairs={{0,2},{2,4},{4,6},{6,0},{1,3},{3,5},{5,7},{7,1},{8,10},{10,12},{12... | collective-permute-start | bytes 786440 | tf_op jit(solution)/shard_map/ppermute | solution.py:37
  118.0 3.6 %collective-permute-start.12 = (bf16[256,512]{1,0:T(8,128)(2,1)S(1)}, bf16[256,512]{1,0:T(8,128)(2,1)S(1)}, u32[]{:S(2)}, u32[]{:S(2)}) collective-permute-start(bf16[256,512]{1,0:T(8,128)(2,1)S(1)} %get-tuple-element.30), channel_id=1, source_target_pairs={{0,4},{2,6},{4,0},{6,2},{1,5},{3,7},{5,1},{7,3},{8,12},{10,14},{12... | collective-permute-start | bytes 786440 | tf_op jit(solution)/shard_map/ppermute | solution.py:37
  121.6 2.4 %collective-permute-done.11.refs_0_ = bf16[256,512]{1,0:T(8,128)(2,1)S(1)} collective-permute-done((bf16[256,512]{1,0:T(8,128)(2,1)S(1)}, bf16[256,512]{1,0:T(8,128)(2,1)S(1)}, u32[]{:S(2)}, u32[]{:S(2)}) %collective-permute-start.11) | collective-permute-done | bytes 262176 | tf_op jit(solution)/shard_map/ppermute | solution.py:37
  123.9 8.7 %collective-permute-start.13 = (bf16[256,512]{1,0:T(8,128)(2,1)S(1)}, bf16[256,512]{1,0:T(8,128)(2,1)S(1)}, u32[]{:S(2)}, u32[]{:S(2)}) collective-permute-start(bf16[256,512]{1,0:T(8,128)(2,1)S(1)} %get-tuple-element.31), channel_id=1, source_target_pairs={{0,6},{2,0},{4,2},{6,4},{1,7},{3,1},{5,3},{7,5},{8,14},{10,8},{12,... | collective-permute-start | bytes 786440 | tf_op jit(solution)/shard_map/ppermute | solution.py:37
  132.6 6.3 %shard_map.164 = (bf16[256,2048]{1,0:T(8,128)(2,1)S(1)}, bf16[128,2048]{1,0:T(8,128)(2,1)S(1)}, bf16[128,2048]{1,0:T(8,128)(2,1)S(1)}, bf16[256,2048]{1,0:T(8,128)(2,1)S(1)}, bf16[256,2048]{1,0:T(8,128)(2,1)S(1)}) custom-call(s32[3]{0:T(128)S(1)} %pad_add_fusion.where_ref.refs_8_, f32[4]{0:T(128)S(1)} %copy-done.8, ...), custom_call_target="tpu_custom_call" | custom-call | flops 738197504 | bytes 4000000 | tf_op jit(solution)/shard_map/pallas_call | solution.py:399
  138.9 5.3 %output.1 = bf16[128,2,2048]{2,1,0:T(2,128)(2,1)} custom-call(s32[3]{0:T(128)S(1)} %pad_add_fusion.where_ref.refs_8_, bf16[256,512]{1,0:T(8,128)(2,1)S(1)} %collective-permute-done.11.refs_0_, bf16[256,512]{1,0:T(8,128)(2,1)S(1)} %collective-permute-done.12.refs_1_, bf16[256,512]{1,0:T(8,128)(2,1)S(1)} %collective-permute-done.13.refs_2_, ...), custom_call_target="tpu_custom_call" | custom-call | flops 1610612736 | bytes 10000000 | tf_op jit(solution)/shard_map/output/pallas_call | solution.py:447
  (66 shorter events, 16.6 us)
Async XLA Ops:
  2.0 42.0 %collective-permute-start.14 = (bf16[128,2048]{1,0:T(8,128)(2,1)}, bf16[128,2048]{1,0:T(8,128)(2,1)}, u32[]{:S(2)}, u32[]{:S(2)}) collective-permute-start(bf16[128,2048]{1,0:T(8,128)(2,1)} %constant_dynamic-slice_fusion.1), channel_id=1, source_target_pairs={{0,4},{2,6},{4,0},{6,2},{1,5},{3,7},{5,1},{7,3},{8,12},{10,14},{12... | collective-permute-start | bytes 1572872 | tf_op jit(solution)/shard_map/ppermute | solution.py:37
  24.1 7.8 %collective-permute-start.6 = (f32[8,512]{1,0:T(8,128)S(1)}, f32[8,512]{1,0:T(8,128)S(1)}, u32[]{:S(2)}, u32[]{:S(2)}) collective-permute-start(f32[8,512]{1,0:T(8,128)S(1)} %reduce_sum.9.m0_ref), channel_id=1, source_target_pairs={{0,6},{2,0},{4,2},{6,4},{1,7},{3,1},{5,3},{7,5},{8,14},{10,8},{12,... | collective-permute-start | bytes 49160 | tf_op jit(solution)/shard_map/ppermute | solution.py:37
  25.5 9.5 %collective-permute-start.7 = (f32[8,512]{1,0:T(8,128)S(1)}, f32[8,512]{1,0:T(8,128)S(1)}, u32[]{:S(2)}, u32[]{:S(2)}) collective-permute-start(f32[8,512]{1,0:T(8,128)S(1)} %reduce_sum.9.m0_ref), channel_id=1, source_target_pairs={{0,4},{2,6},{4,0},{6,2},{1,5},{3,7},{5,1},{7,3},{8,12},{10,14},{12... | collective-permute-start | bytes 49160 | tf_op jit(solution)/shard_map/ppermute | solution.py:37
  26.9 34.1 %copy-start.5 = (f32[2048]{0:T(1024)S(1)}, f32[2048]{0:T(1024)}, u32[]{:S(2)}) copy-start(f32[2048]{0:T(1024)} %param.21) | copy-start | bytes 24580
  29.0 16.3 %collective-permute-start.2 = (bf16[128,2048]{1,0:T(8,128)(2,1)}, bf16[128,2048]{1,0:T(8,128)(2,1)}, u32[]{:S(2)}, u32[]{:S(2)}) collective-permute-start(bf16[128,2048]{1,0:T(8,128)(2,1)} %get-tuple-element.21.refs_0_), channel_id=1, source_target_pairs={{0,2},{2,4},{4,6},{6,0},{1,3},{3,5},{5,7},{7,1},{8,10},{10,12},{12... | collective-permute-start | bytes 1572872 | tf_op jit(solution)/shard_map/ppermute | solution.py:37
  31.6 27.9 %collective-permute-start = (bf16[128,2048]{1,0:T(8,128)(2,1)}, bf16[128,2048]{1,0:T(8,128)(2,1)}, u32[]{:S(2)}, u32[]{:S(2)}) collective-permute-start(bf16[128,2048]{1,0:T(8,128)(2,1)} %get-tuple-element.21.refs_0_), channel_id=1, source_target_pairs={{0,6},{2,0},{4,2},{6,4},{1,7},{3,1},{5,3},{7,5},{8,14},{10,8},{12,... | collective-permute-start | bytes 1572872 | tf_op jit(solution)/shard_map/ppermute | solution.py:37
  31.9 26.0 %collective-permute-start.1 = (bf16[128,2048]{1,0:T(8,128)(2,1)}, bf16[128,2048]{1,0:T(8,128)(2,1)}, u32[]{:S(2)}, u32[]{:S(2)}) collective-permute-start(bf16[128,2048]{1,0:T(8,128)(2,1)} %get-tuple-element.22.refs_1_), channel_id=1, source_target_pairs={{0,6},{2,0},{4,2},{6,4},{1,7},{3,1},{5,3},{7,5},{8,14},{10,8},{12,... | collective-permute-start | bytes 1572872 | tf_op jit(solution)/shard_map/ppermute | solution.py:37
  35.1 7.3 %collective-permute-start.8 = (f32[8,512]{1,0:T(8,128)S(1)}, f32[8,512]{1,0:T(8,128)S(1)}, u32[]{:S(2)}, u32[]{:S(2)}) collective-permute-start(f32[8,512]{1,0:T(8,128)S(1)} %reduce_sum.9.m0_ref), channel_id=1, source_target_pairs={{0,2},{2,4},{4,6},{6,0},{1,3},{3,5},{5,7},{7,1},{8,10},{10,12},{12... | collective-permute-start | bytes 49160 | tf_op jit(solution)/shard_map/ppermute | solution.py:37
  42.3 39.8 %collective-permute-start.16 = (bf16[256,2048]{1,0:T(8,128)(2,1)}, bf16[256,2048]{1,0:T(8,128)(2,1)}, u32[]{:S(2)}, u32[]{:S(2)}) collective-permute-start(bf16[256,2048]{1,0:T(8,128)(2,1)} %constant_dynamic-slice_fusion), channel_id=1, source_target_pairs={{0,2},{2,4},{4,6},{6,0},{1,3},{3,5},{5,7},{7,1},{8,10},{10,12},{12... | collective-permute-start | bytes 3145736 | tf_op jit(solution)/shard_map/ppermute | solution.py:37
  43.9 38.2 %collective-permute-start.17 = (bf16[256,2048]{1,0:T(8,128)(2,1)}, bf16[256,2048]{1,0:T(8,128)(2,1)}, u32[]{:S(2)}, u32[]{:S(2)}) collective-permute-start(bf16[256,2048]{1,0:T(8,128)(2,1)} %constant_dynamic-slice_fusion), channel_id=1, source_target_pairs={{0,6},{2,0},{4,2},{6,4},{1,7},{3,1},{5,3},{7,5},{8,14},{10,8},{12,... | collective-permute-start | bytes 3145736 | tf_op jit(solution)/shard_map/ppermute | solution.py:37
  45.3 35.5 %collective-permute-start.3 = (bf16[128,2048]{1,0:T(8,128)(2,1)}, bf16[128,2048]{1,0:T(8,128)(2,1)}, u32[]{:S(2)}, u32[]{:S(2)}) collective-permute-start(bf16[128,2048]{1,0:T(8,128)(2,1)} %get-tuple-element.22.refs_1_), channel_id=1, source_target_pairs={{0,2},{2,4},{4,6},{6,0},{1,3},{3,5},{5,7},{7,1},{8,10},{10,12},{12... | collective-permute-start | bytes 1572872 | tf_op jit(solution)/shard_map/ppermute | solution.py:37
  57.9 30.6 %collective-permute-start.4 = (bf16[128,2048]{1,0:T(8,128)(2,1)}, bf16[128,2048]{1,0:T(8,128)(2,1)}, u32[]{:S(2)}, u32[]{:S(2)}) collective-permute-start(bf16[128,2048]{1,0:T(8,128)(2,1)} %collective-permute-done.2.refs_4_), channel_id=1, source_target_pairs={{0,2},{2,4},{4,6},{6,0},{1,3},{3,5},{5,7},{7,1},{8,10},{10,12},{12... | collective-permute-start | bytes 1572872 | tf_op jit(solution)/shard_map/ppermute | solution.py:37
  59.5 29.0 %collective-permute-start.5 = (bf16[128,2048]{1,0:T(8,128)(2,1)}, bf16[128,2048]{1,0:T(8,128)(2,1)}, u32[]{:S(2)}, u32[]{:S(2)}) collective-permute-start(bf16[128,2048]{1,0:T(8,128)(2,1)} %collective-permute-done.1.refs_3_), channel_id=1, source_target_pairs={{0,6},{2,0},{4,2},{6,4},{1,7},{3,1},{5,3},{7,5},{8,14},{10,8},{12,... | collective-permute-start | bytes 1572872 | tf_op jit(solution)/shard_map/ppermute | solution.py:37
  64.4 43.3 %all-to-all-start.1 = ((bf16[16,2,64,256]{3,2,1,0:T(8,128)(2,1)}), bf16[16,2,64,256]{3,2,1,0:T(8,128)(2,1)S(1)}, u32[]{:S(2)}, u32[]{:S(2)}) async-start(bf16[16,2,64,256]{3,2,1,0:T(8,128)(2,1)} %get-tuple-element.28), calls=%async_computation.1 | async-start | bytes 2097152 | tf_op jit(solution)/shard_map/all_to_all | solution.py:501
  80.8 37.1 %collective-permute-start.15 = (bf16[128,2048]{1,0:T(8,128)(2,1)}, bf16[128,2048]{1,0:T(8,128)(2,1)}, u32[]{:S(2)}, u32[]{:S(2)}) collective-permute-start(bf16[128,2048]{1,0:T(8,128)(2,1)} %collective-permute-done.14.refs_1_), channel_id=1, source_target_pairs={{0,8},{1,33},{8,0},{9,41},{16,24},{17,49},{24,16},{25,57},{32,40},... | collective-permute-start | bytes 1572872 | tf_op jit(solution)/shard_map/ppermute | solution.py:511
  82.1 56.8 %collective-permute-start.20 = (bf16[256,2048]{1,0:T(8,128)(2,1)}, bf16[256,2048]{1,0:T(8,128)(2,1)}, u32[]{:S(2)}, u32[]{:S(2)}) collective-permute-start(bf16[256,2048]{1,0:T(8,128)(2,1)} %collective-permute-done.16.refs_3_), channel_id=1, source_target_pairs={{0,1},{1,0},{2,3},{3,2},{4,5},{5,4},{6,7},{7,6},{8,9},{9,8},{10,11... | collective-permute-start | bytes 3145736 | tf_op jit(solution)/shard_map/ppermute | solution.py:37
  82.2 56.8 %collective-permute-start.21 = (bf16[256,2048]{1,0:T(8,128)(2,1)}, bf16[256,2048]{1,0:T(8,128)(2,1)}, u32[]{:S(2)}, u32[]{:S(2)}) collective-permute-start(bf16[256,2048]{1,0:T(8,128)(2,1)} %collective-permute-done.17.refs_4_), channel_id=1, source_target_pairs={{0,1},{1,0},{2,3},{3,2},{4,5},{5,4},{6,7},{7,6},{8,9},{9,8},{10,11... | collective-permute-start | bytes 3145736 | tf_op jit(solution)/shard_map/ppermute | solution.py:37
  97.6 7.1 %collective-permute-start.10 = (bf16[2,2,128,128]{3,2,1,0:T(8,128)(2,1)}, bf16[2,2,128,128]{3,2,1,0:T(8,128)(2,1)S(1)}, u32[]{:S(2)}, u32[]{:S(2)}) collective-permute-start(bf16[2,2,128,128]{3,2,1,0:T(8,128)(2,1)} %get-tuple-element.27), channel_id=1, source_target_pairs={{8,0},{16,8},{24,16},{32,24},{40,32},{48,40},{56,48},{64,56},{72,6... | collective-permute-start | bytes 393224 | tf_op jit(solution)/shard_map/ppermute | solution.py:525
  100.6 7.1 %collective-permute-start.9 = (bf16[2,2,128,128]{3,2,1,0:T(8,128)(2,1)}, bf16[2,2,128,128]{3,2,1,0:T(8,128)(2,1)S(1)}, u32[]{:S(2)}, u32[]{:S(2)}) collective-permute-start(bf16[2,2,128,128]{3,2,1,0:T(8,128)(2,1)} %get-tuple-element.26), channel_id=1, source_target_pairs={{0,8},{8,16},{16,24},{24,32},{32,40},{40,48},{48,56},{56,64},{64,7... | collective-permute-start | bytes 393224 | tf_op jit(solution)/shard_map/ppermute | solution.py:524
  104.7 13.3 %collective-permute-start.18 = (bf16[128,2048]{1,0:T(8,128)(2,1)}, bf16[128,2048]{1,0:T(8,128)(2,1)}, u32[]{:S(2)}, u32[]{:S(2)}) collective-permute-start(bf16[128,2048]{1,0:T(8,128)(2,1)} %collective-permute-done.14.refs_1_), channel_id=1, source_target_pairs={{0,1},{1,0},{2,3},{3,2},{4,5},{5,4},{6,7},{7,6},{8,9},{9,8},{10,11... | collective-permute-start | bytes 1572872 | tf_op jit(solution)/shard_map/ppermute | solution.py:37
  116.2 7.8 %collective-permute-start.11 = (bf16[256,512]{1,0:T(8,128)(2,1)S(1)}, bf16[256,512]{1,0:T(8,128)(2,1)S(1)}, u32[]{:S(2)}, u32[]{:S(2)}) collective-permute-start(bf16[256,512]{1,0:T(8,128)(2,1)S(1)} %get-tuple-element.29), channel_id=1, source_target_pairs={{0,2},{2,4},{4,6},{6,0},{1,3},{3,5},{5,7},{7,1},{8,10},{10,12},{12... | collective-permute-start | bytes 786440 | tf_op jit(solution)/shard_map/ppermute | solution.py:37
  118.0 20.9 %collective-permute-start.19 = (bf16[128,2048]{1,0:T(8,128)(2,1)}, bf16[128,2048]{1,0:T(8,128)(2,1)S(1)}, u32[]{:S(2)}, u32[]{:S(2)}) collective-permute-start(bf16[128,2048]{1,0:T(8,128)(2,1)} %collective-permute-done.15.refs_2_), channel_id=1, source_target_pairs={{0,1},{1,0},{2,3},{3,2},{4,5},{5,4},{6,7},{7,6},{8,9},{9,8},{10,11... | collective-permute-start | bytes 1572872 | tf_op jit(solution)/shard_map/ppermute | solution.py:37
  118.0 20.9 %collective-permute-start.12 = (bf16[256,512]{1,0:T(8,128)(2,1)S(1)}, bf16[256,512]{1,0:T(8,128)(2,1)S(1)}, u32[]{:S(2)}, u32[]{:S(2)}) collective-permute-start(bf16[256,512]{1,0:T(8,128)(2,1)S(1)} %get-tuple-element.30), channel_id=1, source_target_pairs={{0,4},{2,6},{4,0},{6,2},{1,5},{3,7},{5,1},{7,3},{8,12},{10,14},{12... | collective-permute-start | bytes 786440 | tf_op jit(solution)/shard_map/ppermute | solution.py:37
  123.9 14.9 %collective-permute-start.13 = (bf16[256,512]{1,0:T(8,128)(2,1)S(1)}, bf16[256,512]{1,0:T(8,128)(2,1)S(1)}, u32[]{:S(2)}, u32[]{:S(2)}) collective-permute-start(bf16[256,512]{1,0:T(8,128)(2,1)S(1)} %get-tuple-element.31), channel_id=1, source_target_pairs={{0,6},{2,0},{4,2},{6,4},{1,7},{3,1},{5,3},{7,5},{8,14},{10,8},{12,... | collective-permute-start | bytes 786440 | tf_op jit(solution)/shard_map/ppermute | solution.py:37
  (14 other events, 233.5 us)
